TPU v7x, 128 devices: a whole 4x4x4 slice. The times are simulated.
128 devices in a mesh: ep: 64 (over z, y, x), tp: 2 (over core).
Axes of the slice: x: 4, y: 4, z: 4, core: 2. Of those that a mesh axis runs over, the one named last changes fastest.
Arguments:
- tokens: bfloat16 [1536, 2048], P('ep'), may hold values from -6 to 6
- norm_gain: bfloat16 [2048], replicated, may hold values from 0.099609375 to 1.8984375
- query_w: bfloat16 [2048, 1024], P(None, 'tp'), may hold values from -0.125 to 0.125
- key_w: bfloat16 [2048, 128], replicated, may hold values from -0.125 to 0.125
- value_w: bfloat16 [2048, 128], replicated, may hold values from -0.125 to 0.125
- forget_w: bfloat16 [2048, 16], replicated, may hold values from -0.125 to 0.125
- forget_bias: float32 [16], replicated, may hold values from 0 to 4
- query_gain: bfloat16 [64], replicated, may hold values from 0.099609375 to 1.8984375
- key_gain: bfloat16 [64], replicated, may hold values from 0.099609375 to 1.8984375
- cache_key: bfloat16 [1536, 2, 64, 1024], P('ep', 'tp'), may hold values from -6 to 6
- cache_value: bfloat16 [1536, 2, 64, 1024], P('ep', 'tp'), may hold values from -6 to 6
- cache_gate: float32 [1536, 16, 1024], P('ep', 'tp'), may hold values from -105 to 0, as said below
- cache_len: int32 [1536], P('ep'), may hold values from 256 to 1024
- out_w: bfloat16 [1024, 2048], P('tp'), may hold values from -0.1875 to 0.1875
- post_gain: bfloat16 [2048], replicated, may hold values from 0.099609375 to 1.8984375
- branch_gate: bfloat16 [2048], replicated, may hold values from -0.125 to 0.125
- dense_gate_w: bfloat16 [2048, 16384], P(None, ('ep', 'tp')), may hold values from -0.125 to 0.125
- dense_up_w: bfloat16 [2048, 16384], P(None, ('ep', 'tp')), may hold values from -1.3258252 to 1.3258252
- dense_down_w: bfloat16 [16384, 2048], P(('ep', 'tp')), may hold values from -0.046875 to 0.046875
- expert_choice: int32 [1536, 2], P('ep'), may hold values from 0 to 63, as said below
- route_weight: float32 [1536, 2], P('ep'), may hold values from 0.1 to 1
- expert_gate_w: bfloat16 [64, 2048, 1024], P('ep', None, 'tp'), may hold values from -0.125 to 0.125
- expert_up_w: bfloat16 [64, 2048, 1024], P('ep', None, 'tp'), may hold values from -0.125 to 0.125
- expert_down_w: bfloat16 [64, 1024, 2048], P('ep', 'tp'), may hold values from -0.1875 to 0.1875
Outputs:
- mixed_out: bfloat16 [1536, 2048], P('ep', 'tp')
- fresh_key: bfloat16 [1536, 2, 64], P('ep', 'tp')
- fresh_value: bfloat16 [1536, 2, 64], P('ep', 'tp')
- fresh_gate: float32 [1536, 16], P('ep', 'tp')
Inputs may be any that keep to these rules, and one draw needn't show every extreme that they name: `cache_gate`: Non-increasing along positions. `expert_choice`: experts 16 * g to 16 * g + 15 form group g. A token names 2 different experts of one group. Among the 24 tokens of one index of ep, those at even offsets all choose one group and the others choose other groups; no expert is named more than 2 times by them, and some expert exactly 2 times.
All inputs are finite; a program needn't handle non-finite values.
Results may differ from a plain program's by a relative error of at most 0.014.
Values may be sent and summed in bfloat16 or wider, within the bound.
A program may use at most 128 MiB of HBM per device.

v0:
```python
import math

import jax
import jax.numpy as jnp
from jax import lax
from jax.sharding import PartitionSpec as P

FF2 = 16384
GROUPS = 4


norm_eps = 1e-06


def sent_to_all(array, axis):
    copies = jnp.broadcast_to(array, (lax.axis_size(axis), *array.shape))
    return lax.all_to_all(copies, axis, split_axis=0, concat_axis=0, tiled=True)


def taken_together(array, axis):
    everything = sent_to_all(array, axis)
    return jnp.sum(everything.astype(jnp.float32), axis=0)


def cut_along(array, dim, size):
    before, after = (array.shape[:dim], array.shape[dim + 1 :])
    return jnp.moveaxis(array.reshape(*before, size, -1, *after), dim, 0)


def summed_on_arrival(array, axis, dim):
    size = lax.axis_size(axis)
    parts = lax.all_to_all(cut_along(array, dim, size), axis, 0, 0, tiled=True)
    return jnp.sum(parts.astype(jnp.float32), axis=0)


def side_by_side(arrays, axis, dim, along):
    widths = [math.prod(a.shape[along:]) for a in arrays]
    both = jnp.concatenate(
        [a.reshape(*a.shape[:along], w) for a, w in zip(arrays, widths)], axis=along
    )
    out = summed_on_arrival(both, axis, dim)
    parts = jnp.split(out, [sum(widths[:k]) for k in range(1, len(widths))], axis=along)
    return tuple((b.reshape(*out.shape[:along], *a.shape[along:]) for a, b in zip(arrays, parts)))


def exchange_in_groups(array, axis, split_dim, concat_dim, work, item_dim, out_dim):

    def moved(group):
        return lax.all_to_all(group, axis, split_axis=split_dim, concat_axis=concat_dim, tiled=True)

    items = jax.tree.leaves(array)[0].shape[item_dim]
    ends = [items * k // 2 for k in range(2 + 1)] if items % 2 == 0 else [0, items]
    groups = [
        jax.tree.map(lambda a: lax.slice_in_dim(a, low, high, axis=item_dim), array)
        for low, high in zip(ends, ends[1:])
    ]
    arrived = [moved(group) for group in groups]
    made = [work(group) for group in arrived]
    return jax.tree.map(lambda *parts: jnp.concatenate(parts, axis=out_dim), *made)


def rms_scale(values, gain_vec):
    mean_square = jnp.mean(values * values, axis=-1, keepdims=True)
    return values * lax.rsqrt(mean_square + norm_eps) * gain_vec


def rounded(values):
    return lax.optimization_barrier(values.astype(jnp.bfloat16)).astype(jnp.float32)


def swiglu_rows(inputs, gate_weight, up_weight):
    gate_value = jnp.dot(inputs, gate_weight, preferred_element_type=jnp.float32)
    up_value = jnp.dot(inputs, up_weight, preferred_element_type=jnp.float32)
    return jax.nn.silu(gate_value) * up_value


def body(
    tokens,
    norm_gain,
    query_w,
    key_w,
    value_w,
    forget_w,
    forget_bias,
    query_gain,
    key_gain,
    cache_key,
    cache_value,
    cache_gate,
    cache_len,
    out_w,
    post_gain,
    branch_gate,
    dense_gate_w,
    dense_up_w,
    dense_down_w,
    expert_choice,
    route_weight,
    expert_gate_w,
    expert_up_w,
    expert_down_w,
):
    seq_count = tokens.shape[0]
    model_width = tokens.shape[1]
    heads_local = cache_gate.shape[1]
    kv_local = cache_key.shape[1]
    head_size = cache_key.shape[2]
    cache_span = cache_key.shape[3]
    tp_count = lax.axis_size("tp")
    ep_count = lax.axis_size("ep")
    tp_rank = lax.axis_index("tp")
    half_width = model_width // tp_count
    score_scale = head_size ** (-0.5)
    resid_in = tokens.astype(jnp.float32)
    normed = rms_scale(resid_in, norm_gain.astype(jnp.float32)).astype(jnp.bfloat16)
    queries = jnp.dot(normed, query_w, preferred_element_type=jnp.float32).reshape(
        seq_count, heads_local, head_size
    )
    queries = rms_scale(queries, query_gain.astype(jnp.float32)).astype(jnp.bfloat16)
    keys_all = jnp.dot(normed, key_w, preferred_element_type=jnp.float32).reshape(
        seq_count, -1, head_size
    )
    keys_all = rms_scale(keys_all, key_gain.astype(jnp.float32)).astype(jnp.bfloat16)
    values_all = (
        jnp.dot(normed, value_w, preferred_element_type=jnp.float32)
        .astype(jnp.bfloat16)
        .reshape(seq_count, -1, head_size)
    )
    fresh_key = lax.dynamic_slice_in_dim(keys_all, tp_rank * kv_local, kv_local, 1)
    fresh_value = lax.dynamic_slice_in_dim(values_all, tp_rank * kv_local, kv_local, 1)
    forget_all = jax.nn.log_sigmoid(
        jnp.dot(normed, forget_w, preferred_element_type=jnp.float32) + forget_bias
    )
    log_forget = lax.dynamic_slice_in_dim(forget_all, tp_rank * heads_local, heads_local, 1)
    repeat = heads_local // kv_local
    grouped = queries.reshape(seq_count, kv_local, repeat, head_size)
    scores = (
        jnp.einsum("sgrd,sgdl->sgrl", grouped, cache_key, preferred_element_type=jnp.float32)
        * score_scale
    )
    own_score = (
        jnp.einsum("sgrd,sgd->sgr", grouped, fresh_key, preferred_element_type=jnp.float32)
        * score_scale
    )
    current_slot_offset = lax.broadcasted_iota(jnp.int32, (seq_count, cache_span), 1)
    at_last = (current_slot_offset == cache_len[:, None] - 1)[:, None, :]
    previous = jnp.sum(jnp.where(at_last, cache_gate, jnp.zeros_like(cache_gate)), axis=2)
    current = previous + log_forget
    decay_bias = (current[:, :, None] - cache_gate).reshape(seq_count, kv_local, repeat, cache_span)
    is_valid = (current_slot_offset < cache_len[:, None])[:, None, None, :]
    logits = jnp.where(is_valid, scores + decay_bias, -jnp.inf)
    top_logit = jnp.maximum(jnp.max(logits, axis=3), own_score)
    weights = jnp.exp(logits - top_logit[..., None])
    own_weight = jnp.exp(own_score - top_logit)
    total_weight = jnp.sum(weights, axis=3) + own_weight
    cache_probs = (weights / total_weight[..., None]).astype(jnp.bfloat16)
    own_prob = (own_weight / total_weight).astype(jnp.bfloat16)
    mixed_heads = jnp.einsum(
        "sgrl,sgdl->sgrd", cache_probs, cache_value, preferred_element_type=jnp.float32
    )
    mixed_heads = (
        mixed_heads
        + own_prob.astype(jnp.float32)[..., None] * fresh_value.astype(jnp.float32)[:, :, None, :]
    )
    attn_heads = mixed_heads.reshape(seq_count, heads_local * head_size).astype(jnp.bfloat16)
    partial_value = jnp.dot(attn_heads, out_w, preferred_element_type=jnp.float32)
    attn_sum = taken_together(partial_value.astype(jnp.bfloat16), "tp").astype(jnp.float32)
    resid_out = rounded(resid_in + attn_sum)
    post_norm = rms_scale(resid_out, post_gain.astype(jnp.float32)).astype(jnp.bfloat16)
    branch = jax.nn.sigmoid(jnp.dot(post_norm, branch_gate, preferred_element_type=jnp.float32))
    gate_grid, up_grid = (
        lax.all_to_all(dense_gate_w, "tp", split_axis=0, concat_axis=1, tiled=True),
        lax.all_to_all(dense_up_w, "tp", split_axis=0, concat_axis=1, tiled=True),
    )
    down_grid = lax.all_to_all(dense_down_w, "tp", split_axis=1, concat_axis=0, tiled=True)
    own_columns = lax.dynamic_slice_in_dim(post_norm, tp_rank * half_width, half_width, 1)
    all_tokens = lax.all_gather(own_columns, "ep", axis=0, tiled=True)
    gate_part = jnp.dot(all_tokens, gate_grid, preferred_element_type=jnp.float32)
    up_part = jnp.dot(all_tokens, up_grid, preferred_element_type=jnp.float32)
    gate_full, up_full = (
        taken_together(gate_part.astype(jnp.bfloat16), "tp").astype(jnp.float32),
        taken_together(up_part.astype(jnp.bfloat16), "tp").astype(jnp.float32),
    )
    hidden = jax.nn.silu(gate_full) * up_full
    squares = jnp.sum(hidden * hidden, axis=1)
    dense_terms = jnp.dot(
        hidden.astype(jnp.bfloat16), down_grid, preferred_element_type=jnp.float32
    )
    dense_sum, square_sum = side_by_side(
        (dense_terms.astype(jnp.bfloat16), squares.astype(jnp.bfloat16)), "ep", 0, 1
    )
    dense_out = rounded(dense_sum * lax.rsqrt(square_sum / FF2 + norm_eps)[:, None])
    per_group = ep_count // GROUPS
    capacity = 2 * ((seq_count + 2 * per_group - 1) // (2 * per_group))
    route_count = expert_choice.shape[1]
    route_ids = expert_choice.reshape(-1)
    member = (route_ids[:, None] == jnp.arange(ep_count)[None, :]).astype(jnp.int32)
    slot_index = jnp.sum((jnp.cumsum(member, axis=0) - member) * member, axis=1)
    target = (route_ids * capacity + slot_index).reshape(seq_count, route_count)
    place_map = (target[:, :, None] == jnp.arange(ep_count * capacity)[None, None, :]).astype(
        jnp.bfloat16
    )
    outgoing = jnp.einsum("skc,sd->cd", place_map, post_norm, preferred_element_type=jnp.float32)
    outgoing = outgoing.astype(jnp.bfloat16).reshape(ep_count, capacity, model_width)

    def expert_work(arrived):
        item_count = arrived.shape[1]
        slot_rows = arrived.reshape(-1, model_width)
        activated = swiglu_rows(slot_rows, expert_gate_w[0], expert_up_w[0]).astype(jnp.bfloat16)
        partial_out = jnp.dot(activated, expert_down_w[0], preferred_element_type=jnp.float32)
        partial_out = partial_out.reshape(ep_count, item_count, model_width)
        halves = summed_on_arrival(partial_out.astype(jnp.bfloat16), "tp", 2)
        return halves.astype(jnp.bfloat16)

    answered = exchange_in_groups(outgoing, "ep", 0, 0, expert_work, 1, 1)
    returned = lax.all_to_all(answered, "ep", split_axis=0, concat_axis=0, tiled=True).reshape(
        ep_count * capacity, half_width
    )
    routed = jnp.einsum("skc,cd->skd", place_map, returned, preferred_element_type=jnp.float32)
    expert_sum = jnp.sum(route_weight[:, :, None] * routed, axis=1)
    resid_columns = lax.dynamic_slice_in_dim(resid_out, tp_rank * half_width, half_width, 1)
    mixed_out = (resid_columns + expert_sum + branch[:, None] * dense_out).astype(jnp.bfloat16)
    return (mixed_out, fresh_key, fresh_value, current)


def solution(mesh):
    placed = (
        P("ep", None),
        P(),
        P(None, "tp"),
        P(),
        P(),
        P(),
        P(),
        P(),
        P(),
        P("ep", "tp", None, None),
        P("ep", "tp", None, None),
        P("ep", "tp", None),
        P("ep"),
        P("tp", None),
        P(),
        P(),
        P(None, ("ep", "tp")),
        P(None, ("ep", "tp")),
        P(("ep", "tp"), None),
        P("ep", None),
        P("ep", None),
        P("ep", None, "tp"),
        P("ep", None, "tp"),
        P("ep", "tp", None),
    )
    return jax.shard_map(
        body,
        mesh=mesh,
        in_specs=placed,
        out_specs=(P("ep", "tp"), P("ep", "tp", None), P("ep", "tp", None), P("ep", "tp")),
        check_vma=False,
    )
```

profile of v0, /device:TPU:0, one launch (start us, length us, event | category | flops | bytes accessed | tf_op | source)
XLA Modules:
  0.0 239.1 jit_solution(10020534700967878836)
XLA Ops:
  26.7 3.4 %all-to-all-start = ((bf16[2,24,2048]{2,1,0:T(8,128)(2,1)}), bf16[2,24,2048]{2,1,0:T(8,128)(2,1)S(1)}, u32[]{:S(2)}, u32[]{:S(2)}) async-start(bf16[2,24,2048]{2,1,0:T(8,128)(2,1)} %broadcast_in_dim.32), calls=%async_computation | async-start | bytes 393216 | tf_op jit(solution)/shard_map/all_to_all | solution.py:17
  32.6 4.2 %all-to-all-start.6 = ((bf16[2,1024,128]{2,1,0:T(8,128)(2,1)}), bf16[2,1024,128]{2,1,0:T(8,128)(2,1)}, u32[]{:S(2)}, u32[]{:S(2)}) async-start(bf16[2,1024,128]{2,1,0:T(8,128)(2,1)} %bitcast.113), calls=%async_computation.6 | async-start | bytes 1048576 | tf_op jit(solution)/shard_map/all_to_all | solution.py:172
  37.5 2.0 copy.107
  40.8 2.2 reshape.219
  43.0 3.1 %fusion.109 = (bf16[64,1,2048]{2,1,0:T(2,128)(2,1)}, bf16[64,1,2048]{2,1,0:T(2,128)(2,1)}) fusion(bf16[64,2,2048]{2,1,0:T(2,128)(2,1)} %reshape.219), kind=kLoop, calls=%fused_computation.137 | loop fusion | bytes 1048576 | tf_op jit(solution)/shard_map/slice | solution.py:54
  46.6 3.1 %reduce.10 = bf16[64,2048]{1,0:T(8,128)(2,1)S(1)} reduce(bf16[64,1,2048]{2,1,0:T(2,128)(2,1)} %get-tuple-element.7, bf16[]{:T(256)} %broadcast.139), dimensions={1}, to_apply=%get-tuple-element.7.reduce_sub_computation | reduce | bytes 524290 | tf_op jit(solution)/shard_map/slice | solution.py:54
  50.6 6.1 %all_to_all.102 = bf16[2,1024,128]{2,1,0:T(8,128)(2,1)} all-to-all(bf16[2,1024,128]{2,1,0:T(8,128)(2,1)} %bitcast.114), channel_id=1, replica_groups=mesh['ep'=64,'tp'=2] {'tp'}, dimensions={0} | all-to-all | bytes 1048576 | tf_op jit(solution)/shard_map/all_to_all | solution.py:173
  56.7 6.1 %all_to_all.103 = bf16[128,2,1024]{0,2,1:T(8,128)(2,1)} all-to-all(bf16[128,2,1024]{0,2,1:T(8,128)(2,1)} %bitcast.110), channel_id=1, replica_groups=mesh['ep'=64,'tp'=2] {'tp'}, dimensions={1} | all-to-all | bytes 1048576 | tf_op jit(solution)/shard_map/all_to_all | solution.py:175
  62.8 11.5 %all-to-all-start.3 = ((bf16[64,2,1024]{2,1,0:T(2,128)(2,1)}), bf16[64,2,1024]{2,1,0:T(2,128)(2,1)S(1)}, u32[]{:S(2)}, u32[]{:S(2)}) async-start(bf16[64,2,1024]{2,1,0:T(2,128)(2,1)} %reshape.233), calls=%async_computation.3 | async-start | bytes 524288 | tf_op jit(solution)/shard_map/all_to_all | solution.py:49
  76.3 2.1 copy.106
  80.4 3.8 %reduce.11 = bf16[64,2048]{1,0:T(8,128)(2,1)} reduce(bf16[64,1,2048]{2,1,0:T(2,128)(2,1)} %get-tuple-element.6, bf16[]{:T(256)} %broadcast.139), dimensions={1}, to_apply=%get-tuple-element.6.reduce_sub_computation | reduce | bytes 524290 | tf_op jit(solution)/shard_map/slice | solution.py:54
  86.1 10.6 %all-to-all-start.1 = ((bf16[64,2,1024]{2,1,0:T(2,128)(2,1)}), bf16[64,2,1024]{2,1,0:T(2,128)(2,1)}, u32[]{:S(2)}, u32[]{:S(2)}) async-start(bf16[64,2,1024]{2,1,0:T(2,128)(2,1)} %reshape.235), calls=%async_computation.1 | async-start | bytes 524288 | tf_op jit(solution)/shard_map/all_to_all | solution.py:49
  97.7 2.3 fusion.10
  99.9 3.4 %convolution_convert_fusion.4 = bf16[64,2048]{1,0:T(8,128)(2,1)S(1)} fusion(bf16[1,512,2048]{2,1,0:T(8,128)(2,1)} %param.47, bf16[1,2048,512]{2,1,0:T(8,128)(2,1)} %param.46, f32[64,512]{1,0:T(8,128)S(1)} %fusion.10, bf16[64,1,2048]{2,1,0:T(2,128)(2,1)} %reshape.234), kind=kOutput, calls=%fused_computation.12 | convolution fusion | flops 268763136 | bytes 4849664 | tf_op jit(solution)/shard_map/dot_general | solution.py:210
  105.9 3.1 %all-to-all-done.1 = bf16[64,2,1024]{2,1,0:T(2,128)(2,1)} async-done(((bf16[64,2,1024]{2,1,0:T(2,128)(2,1)}), bf16[64,2,1024]{2,1,0:T(2,128)(2,1)}, u32[]{:S(2)}, u32[]{:S(2)}) %all-to-all-start.1) | async-done | bytes 262176 | tf_op jit(solution)/shard_map/all_to_all | solution.py:49
  109.0 4.1 %all-to-all-start.4 = ((bf16[2,64,1,1024]{3,1,2,0:T(8,128)(2,1)}), bf16[2,64,1,1024]{3,1,2,0:T(8,128)(2,1)}, u32[]{:S(2)}, u32[]{:S(2)}) async-start(bf16[2,64,1,1024]{3,1,2,0:T(8,128)(2,1)} %bitcast.107), calls=%async_computation.4 | async-start | bytes 524288 | tf_op jit(solution)/shard_map/all_to_all | solution.py:32
  113.1 2.8 %reshape.236 = bf16[64,1,2048]{2,1,0:T(2,128)(2,1)} reshape(bf16[64,2,1024]{2,1,0:T(2,128)(2,1)} %all-to-all-done.1) | data formatting | bytes 524288
  115.9 2.2 fusion.12
  118.1 3.3 %convolution_convert_fusion.5 = bf16[64,2048]{1,0:T(8,128)(2,1)S(1)} fusion(bf16[1,512,2048]{2,1,0:T(8,128)(2,1)} %param.47, bf16[1,2048,512]{2,1,0:T(8,128)(2,1)} %param.46, f32[64,512]{1,0:T(8,128)S(1)} %fusion.12, bf16[64,1,2048]{2,1,0:T(2,128)(2,1)} %reshape.236), kind=kOutput, calls=%fused_computation.13 | convolution fusion | flops 268763136 | bytes 4849664 | tf_op jit(solution)/shard_map/dot_general | solution.py:210
  124.0 3.4 %all-to-all-start.2 = ((bf16[2,64,1,1024]{3,1,2,0:T(8,128)(2,1)}), bf16[2,64,1,1024]{3,1,2,0:T(8,128)(2,1)S(1)}, u32[]{:S(2)}, u32[]{:S(2)}) async-start(bf16[2,64,1,1024]{3,1,2,0:T(8,128)(2,1)} %bitcast.108), calls=%async_computation.2 | async-start | bytes 524288 | tf_op jit(solution)/shard_map/all_to_all | solution.py:32
  131.6 3.0 %convolution_convert_fusion.2 = bf16[1536,256]{1,0:T(8,128)(2,1)S(1)} fusion(bf16[1536,1024]{1,0:T(8,128)(2,1)} %all-gather.2.cloned.1.call-done, bf16[1024,256]{0,1:T(8,128)(2,1)} %bitcast.117), kind=kOutput, calls=%fused_computation.10 | convolution fusion | flops 805699584 | bytes 4456448 | tf_op jit(solution)/shard_map/dot_general | solution.py:178
  135.8 4.6 %all-to-all-start.7 = ((bf16[2,1536,256]{2,1,0:T(8,128)(2,1)}), bf16[2,1536,256]{2,1,0:T(8,128)(2,1)}, u32[]{:S(2)}, u32[]{:S(2)}) async-start(bf16[2,1536,256]{2,1,0:T(8,128)(2,1)} %broadcast_in_dim.33), calls=%async_computation.7 | async-start | bytes 3145728 | tf_op jit(solution)/shard_map/all_to_all | solution.py:17
  140.5 3.9 %convolution_convert_fusion.1 = bf16[1536,256]{1,0:T(8,128)(2,1)} fusion(bf16[1536,1024]{1,0:T(8,128)(2,1)} %all-gather.2.cloned.1.call-done, bf16[1024,256]{0,1:T(8,128)(2,1)} %bitcast.116), kind=kOutput, calls=%fused_computation.9 | convolution fusion | flops 805699584 | bytes 4456448 | tf_op jit(solution)/shard_map/dot_general | solution.py:179
  144.4 2.4 broadcast_in_dim.34
  146.7 4.6 %all-to-all-start.9 = ((bf16[2,1536,256]{2,1,0:T(8,128)(2,1)}), bf16[2,1536,256]{2,1,0:T(8,128)(2,1)}, u32[]{:S(2)}, u32[]{:S(2)}) async-start(bf16[2,1536,256]{2,1,0:T(8,128)(2,1)} %broadcast_in_dim.34), calls=%async_computation.9 | async-start | bytes 3145728 | tf_op jit(solution)/shard_map/all_to_all | solution.py:17
  151.3 3.0 %convert_reduce_fusion.2 = f32[1536,256]{1,0:T(8,128)} fusion(bf16[2,1536,256]{2,1,0:T(8,128)(2,1)} %all-to-all-done.7), kind=kLoop, calls=%fused_computation.8 | loop fusion | flops 1179648 | bytes 3145728 | tf_op jit(solution)/shard_map/reduce_sum | solution.py:22
  154.4 7.2 %all-to-all-start.5 = ((bf16[64,2,1024]{2,1,0:T(2,128)(2,1)}), bf16[64,2,1024]{2,1,0:T(2,128)(2,1)}, u32[]{:S(2)}, u32[]{:S(2)}) async-start(bf16[64,2,1024]{2,1,0:T(2,128)(2,1)} %copy.104), calls=%async_computation.5 | async-start | bytes 524288 | tf_op jit(solution)/shard_map/all_to_all | solution.py:216
  164.6 2.7 %convolution_convert_fusion = bf16[1536,1024]{1,0:T(8,128)(2,1)} fusion(bf16[256,1024]{1,0:T(8,128)(2,1)S(1)} %bitcast.115, f32[1536,256]{1,0:T(8,128)S(1)} %convert_reduce_fusion.1, f32[1536,256]{1,0:T(8,128)S(1)} %copy-done.1), kind=kOutput, calls=%fused_computation.1 | convolution fusion | flops 809238528 | bytes 6815744 | tf_op jit(solution)/shard_map/dot_general | solution.py:186
  168.0 4.0 %pad_maximum_fusion = bf16[64,24,1025]{2,1,0:T(8,128)(2,1)} fusion(bf16[64,24,1]{2,1,0:T(8,128)(2,1)S(1)} %convert_element_type.177, bf16[64,24,1024]{2,1,0:T(8,128)(2,1)} %bitcast.109), kind=kLoop, calls=%fused_computation.2 | loop fusion | flops 6297600 | bytes 6297600 | tf_op jit(solution)/shard_map/concatenate | solution.py:38
  172.7 10.0 %all-to-all-start.11 = ((bf16[64,24,1025]{2,1,0:T(8,128)(2,1)}), bf16[64,24,1025]{2,1,0:T(8,128)(2,1)}, u32[]{:S(2)}, u32[]{:S(2)}) async-start(bf16[64,24,1025]{2,1,0:T(8,128)(2,1)} %pad_maximum_fusion), calls=%async_computation.11 | async-start | bytes 7077888 | tf_op jit(solution)/shard_map/all_to_all | solution.py:32
  185.6 43.2 %all-to-all-done.11 = bf16[64,24,1025]{2,1,0:T(8,128)(2,1)} async-done(((bf16[64,24,1025]{2,1,0:T(8,128)(2,1)}), bf16[64,24,1025]{2,1,0:T(8,128)(2,1)}, u32[]{:S(2)}, u32[]{:S(2)}) %all-to-all-start.11) | async-done | bytes 3148832 | tf_op jit(solution)/shard_map/all_to_all | solution.py:32
  228.8 2.5 %convert_reduce_fusion = f32[24,1025]{1,0:T(8,128)S(1)} fusion(bf16[64,24,1025]{2,1,0:T(8,128)(2,1)} %all-to-all-done.11), kind=kLoop, calls=%fused_computation | loop fusion | flops 3124200 | bytes 3247200 | tf_op jit(solution)/shard_map/reduce_sum | solution.py:33
  (139 shorter events, 50.5 us)
Async XLA Ops:
  7.2 13.4 %copy-start = (bf16[24,1,64,1024]{3,2,1,0:T(8,128)(2,1)S(1)}, bf16[24,1,64,1024]{3,2,1,0:T(8,128)(2,1)}, u32[]{:S(2)}) copy-start(bf16[24,1,64,1024]{3,2,1,0:T(8,128)(2,1)} %param.33) | copy-start | bytes 9437188
  7.2 10.0 %copy-start.2 = (bf16[24,2048]{1,0:T(8,128)(2,1)S(1)}, bf16[24,2048]{1,0:T(8,128)(2,1)}, u32[]{:S(2)}) copy-start(bf16[24,2048]{1,0:T(8,128)(2,1)} %param.24) | copy-start | bytes 294916
  7.2 10.0 %copy-start.22 = (f32[16]{0:T(128)S(1)}, f32[16]{0:T(128)}, u32[]{:S(2)}) copy-start(f32[16]{0:T(128)} %param.30) | copy-start | bytes 196
  7.2 10.0 %copy-start.21 = (bf16[2048,16]{0,1:T(8,128)(2,1)S(1)}, bf16[2048,16]{0,1:T(8,128)(2,1)}, u32[]{:S(2)}) copy-start(bf16[2048,16]{0,1:T(8,128)(2,1)} %param.29) | copy-start | bytes 196612
  10.2 10.0 %copy-start.15 = (f32[64]{0:T(128)}, f32[64]{0:T(128)S(1)}, u32[]{:S(2)}) copy-start(f32[64]{0:T(128)S(1)} %convert_element_type.143) | copy-start | bytes 772
  15.7 6.9 %copy-start.17 = (f32[24,1]{0,1:T(1,128)}, f32[24,1]{0,1:T(1,128)S(1)}, u32[]{:S(2)}) copy-start(f32[24,1]{0,1:T(1,128)S(1)} %constant_dynamic-slice_fusion.3) | copy-start | bytes 292
  20.6 2.3 copy-start.20
  23.8 6.3 %copy-start.12 = (bf16[2048]{0:T(1024)(128)(2,1)S(1)}, bf16[2048]{0:T(1024)(128)(2,1)}, u32[]{:S(2)}) copy-start(bf16[2048]{0:T(1024)(128)(2,1)} %param.38) | copy-start | bytes 12292
  24.0 12.8 %copy-start.14 = (s32[24,2]{0,1:T(2,128)S(1)}, s32[24,2]{0,1:T(2,128)}, u32[]{:S(2)}) copy-start(s32[24,2]{0,1:T(2,128)} %param.43) | copy-start | bytes 580
  26.7 4.9 %all-to-all-start = ((bf16[2,24,2048]{2,1,0:T(8,128)(2,1)}), bf16[2,24,2048]{2,1,0:T(8,128)(2,1)S(1)}, u32[]{:S(2)}, u32[]{:S(2)}) async-start(bf16[2,24,2048]{2,1,0:T(8,128)(2,1)} %broadcast_in_dim.32), calls=%async_computation | async-start | bytes 393216 | tf_op jit(solution)/shard_map/all_to_all | solution.py:17
  30.1 101.5 %all-gather.2.cloned.1.call-start = ((), (), s32[]{:S(2)}) async-start(), calls=%async_computation.12 | async-start | bytes 3194880 | tf_op jit(solution)/shard_map/all_gather | solution.py:177
  31.6 11.3 %copy-start.3 = (bf16[24,2048]{1,0:T(8,128)(2,1)}, bf16[24,2048]{1,0:T(8,128)(2,1)S(1)}, u32[]{:S(2)}) copy-start(bf16[24,2048]{1,0:T(8,128)(2,1)S(1)} %fusion.64) | copy-start | bytes 294916
  31.9 14.2 %copy-start.5 = (bf16[24,2048]{1,0:T(8,128)(2,1)}, bf16[24,2048]{1,0:T(8,128)(2,1)S(1)}, u32[]{:S(2)}) copy-start(bf16[24,2048]{1,0:T(8,128)(2,1)S(1)} %multiply_convert_fusion) | copy-start | bytes 294916
  32.6 18.0 %all-to-all-start.6 = ((bf16[2,1024,128]{2,1,0:T(8,128)(2,1)}), bf16[2,1024,128]{2,1,0:T(8,128)(2,1)}, u32[]{:S(2)}, u32[]{:S(2)}) async-start(bf16[2,1024,128]{2,1,0:T(8,128)(2,1)} %bitcast.113), calls=%async_computation.6 | async-start | bytes 1048576 | tf_op jit(solution)/shard_map/all_to_all | solution.py:172
  39.6 6.5 %copy-start.10 = (s32[24,2]{0,1:T(2,128)}, s32[24,2]{0,1:T(2,128)S(1)}, u32[]{:S(2)}) copy-start(s32[24,2]{0,1:T(2,128)S(1)} %multiply_add_fusion) | copy-start | bytes 580
  62.8 23.4 %all-to-all-start.3 = ((bf16[64,2,1024]{2,1,0:T(2,128)(2,1)}), bf16[64,2,1024]{2,1,0:T(2,128)(2,1)S(1)}, u32[]{:S(2)}, u32[]{:S(2)}) async-start(bf16[64,2,1024]{2,1,0:T(2,128)(2,1)} %reshape.233), calls=%async_computation.3 | async-start | bytes 524288 | tf_op jit(solution)/shard_map/all_to_all | solution.py:49
  86.1 22.9 %all-to-all-start.1 = ((bf16[64,2,1024]{2,1,0:T(2,128)(2,1)}), bf16[64,2,1024]{2,1,0:T(2,128)(2,1)}, u32[]{:S(2)}, u32[]{:S(2)}) async-start(bf16[64,2,1024]{2,1,0:T(2,128)(2,1)} %reshape.235), calls=%async_computation.1 | async-start | bytes 524288 | tf_op jit(solution)/shard_map/all_to_all | solution.py:49
  109.0 15.0 %all-to-all-start.4 = ((bf16[2,64,1,1024]{3,1,2,0:T(8,128)(2,1)}), bf16[2,64,1,1024]{3,1,2,0:T(8,128)(2,1)}, u32[]{:S(2)}, u32[]{:S(2)}) async-start(bf16[2,64,1,1024]{3,1,2,0:T(8,128)(2,1)} %bitcast.107), calls=%async_computation.4 | async-start | bytes 524288 | tf_op jit(solution)/shard_map/all_to_all | solution.py:32
  124.0 5.0 %all-to-all-start.2 = ((bf16[2,64,1,1024]{3,1,2,0:T(8,128)(2,1)}), bf16[2,64,1,1024]{3,1,2,0:T(8,128)(2,1)S(1)}, u32[]{:S(2)}, u32[]{:S(2)}) async-start(bf16[2,64,1,1024]{3,1,2,0:T(8,128)(2,1)} %bitcast.108), calls=%async_computation.2 | async-start | bytes 524288 | tf_op jit(solution)/shard_map/all_to_all | solution.py:32
  135.8 8.5 %all-to-all-start.7 = ((bf16[2,1536,256]{2,1,0:T(8,128)(2,1)}), bf16[2,1536,256]{2,1,0:T(8,128)(2,1)}, u32[]{:S(2)}, u32[]{:S(2)}) async-start(bf16[2,1536,256]{2,1,0:T(8,128)(2,1)} %broadcast_in_dim.33), calls=%async_computation.7 | async-start | bytes 3145728 | tf_op jit(solution)/shard_map/all_to_all | solution.py:17
  146.7 7.6 %all-to-all-start.9 = ((bf16[2,1536,256]{2,1,0:T(8,128)(2,1)}), bf16[2,1536,256]{2,1,0:T(8,128)(2,1)}, u32[]{:S(2)}, u32[]{:S(2)}) async-start(bf16[2,1536,256]{2,1,0:T(8,128)(2,1)} %broadcast_in_dim.34), calls=%async_computation.9 | async-start | bytes 3145728 | tf_op jit(solution)/shard_map/all_to_all | solution.py:17
  154.4 18.4 %all-to-all-start.5 = ((bf16[64,2,1024]{2,1,0:T(2,128)(2,1)}), bf16[64,2,1024]{2,1,0:T(2,128)(2,1)}, u32[]{:S(2)}, u32[]{:S(2)}) async-start(bf16[64,2,1024]{2,1,0:T(2,128)(2,1)} %copy.104), calls=%async_computation.5 | async-start | bytes 524288 | tf_op jit(solution)/shard_map/all_to_all | solution.py:216
  161.6 2.0 copy-start.1
  172.0 10.7 %copy-start.4 = (bf16[24,2048]{1,0:T(8,128)(2,1)S(1)}, bf16[24,2048]{1,0:T(8,128)(2,1)}, u32[]{:S(2)}) copy-start(bf16[24,2048]{1,0:T(8,128)(2,1)} %copy-done.3) | copy-start | bytes 294916
  172.0 11.4 %copy-start.13 = (bf16[2048]{0:T(1024)(128)(2,1)S(1)}, bf16[2048]{0:T(1024)(128)(2,1)}, u32[]{:S(2)}) copy-start(bf16[2048]{0:T(1024)(128)(2,1)} %param.39) | copy-start | bytes 12292
  172.0 11.4 %copy-start.16 = (f32[64]{0:T(128)S(1)}, f32[64]{0:T(128)}, u32[]{:S(2)}) copy-start(f32[64]{0:T(128)} %copy-done.15) | copy-start | bytes 772
  172.0 11.4 %copy-start.18 = (f32[24,1]{0,1:T(1,128)S(1)}, f32[24,1]{0,1:T(1,128)}, u32[]{:S(2)}) copy-start(f32[24,1]{0,1:T(1,128)} %copy-done.17) | copy-start | bytes 292
  172.1 12.1 %copy-start.6 = (bf16[24,2048]{1,0:T(8,128)(2,1)S(1)}, bf16[24,2048]{1,0:T(8,128)(2,1)}, u32[]{:S(2)}) copy-start(bf16[24,2048]{1,0:T(8,128)(2,1)} %copy-done.5) | copy-start | bytes 294916
  172.1 13.3 %copy-start.11 = (s32[24,2]{0,1:T(2,128)S(1)}, s32[24,2]{0,1:T(2,128)}, u32[]{:S(2)}) copy-start(s32[24,2]{0,1:T(2,128)} %copy-done.10) | copy-start | bytes 580
  172.1 13.3 %copy-start.19 = (f32[24,2]{0,1:T(2,128)S(1)}, f32[24,2]{0,1:T(2,128)}, u32[]{:S(2)}) copy-start(f32[24,2]{0,1:T(2,128)} %param.44) | copy-start | bytes 580
  172.7 56.1 %all-to-all-start.11 = ((bf16[64,24,1025]{2,1,0:T(8,128)(2,1)}), bf16[64,24,1025]{2,1,0:T(8,128)(2,1)}, u32[]{:S(2)}, u32[]{:S(2)}) async-start(bf16[64,24,1025]{2,1,0:T(8,128)(2,1)} %pad_maximum_fusion), calls=%async_computation.11 | async-start | bytes 7077888 | tf_op jit(solution)/shard_map/all_to_all | solution.py:32
  185.6 45.9 %copy-start.8 = (f32[24,2048]{1,0:T(8,128)S(1)}, f32[24,2048]{1,0:T(8,128)}, u32[]{:S(2)}) copy-start(f32[24,2048]{1,0:T(8,128)} %convert_element_type.154) | copy-start | bytes 589828
  (2 other events, 1.6 us)
Sparse Core Ops, SparseCore 0:
  34.2 72.2 all-gather.1
where the time goes:
time: 241 us; the launch traced here: 239 us
  starting transfers between devices  63.8 us (26%)
  waiting for transfers between devices  48.9 us (20%)
  local copies, waits for them, and re-layouts  35.5 us (15%)
  matrix products  32.2 us (13%)
  other arithmetic  31.9 us (13%)
  between operations  14.6 us (6%)
  blocking collectives  12.1 us (5%)
    all_to_all x3, waiting for transfers between devices, summed_on_arrival(): parts = lax.all_to_all(cut_along(array, dim, size), axis, 0, 0, tiled=True)  43.7 us
    all_to_all x2, starting transfers between devices, moved(): lax.all_to_all(group, axis, split_axis=split_dim, concat_axis=concat_dim,...  22.1 us
    all_to_all x3, starting transfers between devices, summed_on_arrival(): parts = lax.all_to_all(cut_along(array, dim, size), axis, 0, 0, tiled=True)  17.6 us
    all_to_all x3, starting transfers between devices, sent_to_all(): return lax.all_to_all(copies, axis, split_axis=0, concat_axis=0, tiled=True)  12.6 us
    unnamed x53, local copies, waits for them, and re-layouts  9.71 us
    all_to_all x1, starting transfers between devices, body(): lax.all_to_all(answered, 'ep', split_axis=0, concat_axis=0, tiled=True)  7.25 us
    slice x2, other arithmetic, exchange_in_groups(): lax.slice_in_dim(a, low, high, axis=item_dim)  6.96 us
    dot_general x2, matrix products, expert_work(): jnp.dot(activated, expert_down_w[0], preferred_element_type=jnp.float32)  6.66 us
  transfers between devices with their start and end apart: 11, of which 5 were waited for; matrix products, arithmetic and copies ran while one was open for 29% of the time, Pallas kernels for 0%

commit v1 on v0

v1 whole, which is shorter than its diff:
```python
import math
import functools

import jax
import jax.numpy as jnp
from jax import lax
from jax.experimental import pallas as pl
from jax.experimental.pallas import tpu as pltpu
from jax.sharding import PartitionSpec as P

FF2 = 16384
norm_eps = 1e-06
MESH = pl.DeviceIdType.MESH
f32, bf16 = jnp.float32, jnp.bfloat16


class Sems:
    def __init__(self, send, recv):
        self.send, self.recv, self.n = send, recv, 0
        self.sent = []

    def copy(self, src, dst, device):
        i = self.n
        self.n += 1
        cp = pltpu.make_async_remote_copy(
            src_ref=src,
            dst_ref=dst,
            send_sem=self.send.at[i],
            recv_sem=self.recv.at[i],
            device_id=device,
            device_id_type=MESH,
        )
        cp.start()
        self.sent.append(cp)
        return cp


def silu(v):
    return v / (1.0 + jnp.exp(-v))


def layer_kernel(
    partial_ref, tokens_ref, gain_ref, bgate_ref, meta_ref, comb_ref,
    dg_h, du_h, dd_h, eg_h, eu_h, ed_h,
    out_ref,
    partner_part, resid_s, pn_s, a1, xs, hid, wgu, wd, eg, eu, ed,
    meta_all, meta_tab, xg, dens, rl, rr, ql, qr, sl, sr, t2, r2, t3, r3,
    sq, sq1, sq2, sq2r, sq3, sq3r, ep_send, ep_recv, ret_f, ret_b, back,
    send_sem, recv_sem, load_sem, meta_sems, back_sems,
):
    me = lax.axis_index("ep")
    core = lax.axis_index("tp")
    other = 1 - core
    coords = (me % 4, (me // 4) % 4, me // 16)
    weights = (1, 4, 16)
    partner = (me, other)
    half = pl.multiple_of(core * 1024, 1024)
    ohalf = pl.multiple_of(other * 1024, 1024)
    ccol = pl.multiple_of(core * 128, 128)

    def peer(dim, k):
        v = coords[dim]
        return (me + (((v + k) % 4) - v) * weights[dim], core)

    sems = Sems(send_sem, recv_sem)

    loads = []
    for i, (src, dst) in enumerate((
        (dg_h, wgu.at[:, pl.ds(0, 128)]),
        (du_h, wgu.at[:, pl.ds(128, 128)]),
        (dd_h.at[:, pl.ds(half, 1024)], wd.at[pl.ds(ccol, 128)]),
        (eg_h, eg),
        (eu_h, eu),
        (ed_h, ed),
    )):
        cp = pltpu.make_async_copy(src, dst, load_sem.at[i])
        cp.start()
        loads.append(cp)

    barrier = pltpu.get_barrier_semaphore()
    pl.semaphore_signal(barrier, inc=1, device_id=partner, device_id_type=MESH)

    @pl.loop(1, 64)
    def _(i):
        pl.semaphore_signal(
            barrier, inc=1, device_id=((me + i) % 64, core), device_id_type=MESH
        )

    pl.semaphore_wait(barrier, 64)

    part_cp = sems.copy(partial_ref, partner_part, partner)
    wd_cp = sems.copy(dd_h.at[:, pl.ds(ohalf, 1024)], wd.at[pl.ds(ccol, 128)], partner)

    def meta_copy(d):
        return pltpu.make_async_remote_copy(
            src_ref=meta_ref,
            dst_ref=meta_all.at[me],
            send_sem=meta_sems.at[0],
            recv_sem=meta_sems.at[1],
            device_id=(d, core),
            device_id_type=MESH,
        )

    part_cp.wait_recv()
    attn = partial_ref[...].astype(f32) + partner_part[...].astype(f32)
    resid = (tokens_ref[...].astype(f32) + attn).astype(bf16).astype(f32)
    resid_s[...] = resid
    mean_square = jnp.mean(resid * resid, axis=-1, keepdims=True)
    gain = gain_ref[...].astype(f32)[None]
    post = (resid * lax.rsqrt(mean_square + norm_eps) * gain).astype(bf16)
    pn_s[...] = post
    a1[:, 0] = pn_s[:, :, pl.ds(half, 1024)]

    g1 = [
        [sems.copy(a1.at[p, 0], a1.at[p, 4 - k], peer(p, k)) for k in (1, 3, 2)]
        for p in range(3)
    ]

    @pl.loop(1, 64)
    def _(i):
        meta_copy((me + i) % 64).start()

    meta_all[me] = meta_ref[...]
    branch = jax.nn.sigmoid(
        jnp.sum(post.astype(f32) * bgate_ref[...].astype(f32)[None], axis=-1, keepdims=True)
    )

    g2 = []
    for p in range(3):
        for cp in g1[p]:
            cp.wait_recv()
        for pair in range(2):
            rows = jnp.concatenate(
                [a1[p, 2 * pair].astype(f32), a1[p, 2 * pair + 1].astype(f32)], axis=0
            )
            xs[core, 0, pl.ds(p * 128 + pair * 16, 16)] = rows.astype(bf16)
        line = xs.at[core, 0, pl.ds(p * 128, 32)]
        g2.append([
            sems.copy(line, xs.at[core, 0, pl.ds(p * 128 + (4 - k) * 32, 32)], peer((p + 1) % 3, k))
            for k in (1, 3, 2)
        ])

    g3, d2d = [], [[] for _ in range(4)]

    def share(slot, p, start, size):
        view = xs.at[core, slot, pl.ds(p * 128 + start, size)]
        d2d[slot].append(sems.copy(view, view, partner))

    for p in range(3):
        for cp in g2[p]:
            cp.wait_recv()
        cdim = (p + 2) % 3
        rows = pl.ds(p * 128, 128)
        g3.append((
            sems.copy(xs.at[core, 0, rows], xs.at[core, 1, rows], peer(cdim, 1)),
            sems.copy(xs.at[core, 0, rows], xs.at[core, 2, rows], peer(cdim, 3)),
        ))
        share(0, p, 0, 128)

    pltpu.make_async_copy(
        meta_all.at[pl.ds(0, 63)], meta_all.at[pl.ds(0, 63)], meta_sems.at[1]
    ).wait()
    for d in range(64):
        meta_tab[pl.ds(d, 1), :] = meta_all[d]
    table = meta_tab[...]
    lane = lax.broadcasted_iota(jnp.int32, (64, 128), 1)
    dev = lax.broadcasted_iota(jnp.int32, (64, 1), 0)
    shift = [((dev >> s) - coords[i]) & 3 for i, s in enumerate((0, 2, 4))]
    starts = []
    for p in range(3):
        ka, kb, kc = shift[p], shift[(p + 1) % 3], shift[(p + 2) % 3]
        slot = jnp.where(kc == 0, 0, jnp.where(kc == 1, 2, jnp.where(kc == 2, 3, 1)))
        starts.append(slot * 384 + p * 128 + kb * 32 + ka * 8)
    row_ids = []
    for s in range(2):
        want = (me * 2 + s).astype(f32)
        tok = jnp.sum(jnp.where(table == want, (lane >> 1) + 1, 0), axis=1, keepdims=True) - 1
        start = jnp.where(tok < 8, starts[0], jnp.where(tok < 16, starts[1], starts[2]))
        row_ids.append(jnp.where(tok < 0, -1, start + (tok & 7)))
    row_id = jnp.concatenate(row_ids, axis=0)
    cols = lax.broadcasted_iota(jnp.int32, (128, 384), 1)

    def select(slot):
        pick = jnp.where(row_id == cols + slot * 384, 1.0, 0.0).astype(bf16)
        for h in range(2):
            got = jnp.dot(pick, xs[h, slot], preferred_element_type=f32)
            if slot:
                got = xg[h] + got
            xg[h] = got

    h_cp = [None] * 4

    def up_proj(slot):
        v = jnp.dot(xs[0, slot], wgu[pl.ds(0, 1024)], preferred_element_type=f32)
        v = v + jnp.dot(xs[1, slot], wgu[pl.ds(1024, 1024)], preferred_element_type=f32)
        hid[slot, :, pl.ds(ccol, 128)] = (silu(v[:, :128]) * v[:, 128:]).astype(bf16)
        view = hid.at[slot, :, pl.ds(ccol, 128)]
        h_cp[slot] = sems.copy(view, view, partner)

    ones = jnp.ones((8, 256), bf16)

    def down_proj(slot):
        h_cp[slot].wait_recv()
        h = hid[slot]
        hf = h.astype(f32)
        dens[slot] = jnp.dot(h, wd[...], preferred_element_type=f32).astype(bf16)
        s = lax.dot_general(
            ones, (hf * hf).astype(bf16), (((1,), (1,)), ((), ())), preferred_element_type=f32
        )
        for p in range(3):
            sq[slot, p] = s[0:1, p * 128:(p + 1) * 128]

    def arrive(slot):
        for cp in d2d[slot]:
            cp.wait_recv()

    loads[0].wait()
    loads[1].wait()
    arrive(0)
    up_proj(0)
    select(0)

    relay = []
    for p in range(3):
        cdim = (p + 2) % 3
        g3[p][0].wait_recv()
        rows = pl.ds(p * 128, 64)
        relay.append(sems.copy(xs.at[core, 1, rows], xs.at[core, 3, rows], peer(cdim, 1)))
        share(1, p, 0, 128)
        g3[p][1].wait_recv()
        rows = pl.ds(p * 128 + 64, 64)
        relay.append(sems.copy(xs.at[core, 2, rows], xs.at[core, 3, rows], peer(cdim, 3)))
        share(2, p, 0, 128)

    arrive(1)
    up_proj(1)
    arrive(2)
    up_proj(2)
    loads[2].wait()
    wd_cp.wait_recv()
    select(1)
    down_proj(1)
    select(2)
    down_proj(2)

    s1 = []
    for p in range(3):
        cdim = (p + 2) % 3
        s1.append([
            sems.copy(dens.at[2, pl.ds(p * 128 + 64, 64)], rl.at[p, 1], peer(cdim, 1)),
            sems.copy(dens.at[1, pl.ds(p * 128, 64)], rr.at[p, 0], peer(cdim, 3)),
        ])

    for p in range(3):
        relay[2 * p].wait_recv()
        share(3, p, 0, 64)
        relay[2 * p + 1].wait_recv()
        share(3, p, 64, 64)
    arrive(3)
    up_proj(3)
    select(3)
    down_proj(3)
    far = []
    for p in range(3):
        cdim = (p + 2) % 3
        far.append((
            sems.copy(dens.at[3, pl.ds(p * 128, 64)], ql.at[p], peer(cdim, 1)),
            sems.copy(dens.at[3, pl.ds(p * 128 + 64, 64)], qr.at[p], peer(cdim, 3)),
        ))
        s1[p] += [
            sems.copy(sq.at[2, p], sq1.at[p, 0], peer(cdim, 1)),
            sems.copy(sq.at[1, p], sq1.at[p, 1], peer(cdim, 3)),
            sems.copy(sq.at[3, p], sq1.at[p, 2], peer(cdim, 2)),
        ]

    for i in (3, 4, 5):
        loads[i].wait()
    x0, x1 = xg[0].astype(bf16), xg[1].astype(bf16)
    gate = jnp.dot(x0, eg[pl.ds(0, 1024)], preferred_element_type=f32)
    gate = gate + jnp.dot(x1, eg[pl.ds(1024, 1024)], preferred_element_type=f32)
    up = jnp.dot(x0, eu[pl.ds(0, 1024)], preferred_element_type=f32)
    up = up + jnp.dot(x1, eu[pl.ds(1024, 1024)], preferred_element_type=f32)
    act = (silu(gate) * up).astype(bf16)
    ep_send[...] = jnp.dot(act, ed[:, pl.ds(ohalf, 1024)], preferred_element_type=f32).astype(bf16)
    ep_cp = sems.copy(ep_send, ep_recv, partner)
    mine = jnp.dot(act, ed[:, pl.ds(half, 1024)], preferred_element_type=f32).astype(bf16)

    for p in range(3):
        cdim = (p + 2) % 3
        far[p][0].wait_recv()
        sl[p] = (dens[2, pl.ds(p * 128, 64)].astype(f32) + ql[p].astype(f32)).astype(bf16)
        s1[p].append(sems.copy(sl.at[p], rl.at[p, 0], peer(cdim, 1)))
        far[p][1].wait_recv()
        sr[p] = (dens[1, pl.ds(p * 128 + 64, 64)].astype(f32) + qr[p].astype(f32)).astype(bf16)
        s1[p].append(sems.copy(sr.at[p], rr.at[p, 1], peer(cdim, 3)))

    ep_cp.wait_recv()
    rows = (mine.astype(f32) + ep_recv[...].astype(f32)).astype(bf16).astype(f32)
    for s in range(2):
        for t in range(8):
            ret_f[pl.ds(s * 8 + t, 64, stride=16), :] = rows[s * 64:(s + 1) * 64, t * 128:(t + 1) * 128]
    ret_b[...] = ret_f[...].astype(bf16).reshape(64, 16, 128)

    def back_copy(d):
        return pltpu.make_async_remote_copy(
            src_ref=ret_b.at[d],
            dst_ref=back.at[me],
            send_sem=back_sems.at[0],
            recv_sem=back_sems.at[1],
            device_id=(d, core),
            device_id_type=MESH,
        )

    @pl.loop(1, 64)
    def _(i):
        back_copy((me + i) % 64).start()

    back[me] = ret_b[me]
    down_proj(0)

    s2 = []
    for p in range(3):
        for cp in s1[p]:
            cp.wait_recv()
        total = dens[0, pl.ds(p * 128, 128)].astype(f32)
        total = total + jnp.concatenate([rl[p, 0], rl[p, 1]], axis=0).astype(f32)
        total = total + jnp.concatenate([rr[p, 0], rr[p, 1]], axis=0).astype(f32)
        for k in range(4):
            t2[p, k] = total[k * 32:(k + 1) * 32].astype(bf16)
        v = sq[0, p] + sq1[p, 0] + sq1[p, 1] + sq1[p, 2]
        sq2[p, 0] = v
        for k in range(1, 4):
            sq2[p, k] = pltpu.roll(v, 128 - 32 * k, 1)
        s2.append([
            sems.copy(t2.at[p, k], r2.at[p, k - 1], peer((p + 1) % 3, k)) for k in (1, 3, 2)
        ] + [
            sems.copy(sq2.at[p, k], sq2r.at[p, k - 1], peer((p + 1) % 3, k)) for k in (1, 3, 2)
        ])

    pltpu.make_async_copy(back.at[pl.ds(0, 63)], back.at[pl.ds(0, 63)], back_sems.at[1]).wait()
    ret_f[...] = back[...].reshape(1024, 128).astype(f32)
    mixes = []
    for t in range(8):
        m = 0.0
        for s in range(2):
            m = m + jnp.dot(
                comb_ref[s], ret_f[pl.ds(s * 8 + t, 64, stride=16), :],
                preferred_element_type=f32, precision=lax.Precision.HIGHEST,
            )
        mixes.append(m)
    expert_sum = jnp.concatenate(mixes, axis=1)

    s3 = []
    for p in range(3):
        for cp in s2[p]:
            cp.wait_recv()
        total = t2[p, 0].astype(f32)
        for k in range(3):
            total = total + r2[p, k].astype(f32)
        for k in range(4):
            t3[p, k] = total[k * 8:(k + 1) * 8].astype(bf16)
        v = sq2[p, 0] + sq2r[p, 0] + sq2r[p, 1] + sq2r[p, 2]
        sq3[p, 0] = v
        for k in range(1, 4):
            sq3[p, k] = pltpu.roll(v, 128 - 8 * k, 1)
        s3.append([
            sems.copy(t3.at[p, k], r3.at[p, k - 1], peer(p, k)) for k in (1, 3, 2)
        ] + [
            sems.copy(sq3.at[p, k], sq3r.at[p, k - 1], peer(p, k)) for k in (1, 3, 2)
        ])

    eye = lax.broadcasted_iota(jnp.int32, (8, 128), 0) == lax.broadcasted_iota(jnp.int32, (8, 128), 1)
    for p in range(3):
        for cp in s3[p]:
            cp.wait_recv()
        total = t3[p, 0].astype(f32)
        v = sq3[p, 0]
        for k in range(3):
            total = total + r3[p, k].astype(f32)
            v = v + sq3r[p, k]
        square = jnp.sum(jnp.where(eye, v, 0.0), axis=1, keepdims=True)
        dense = (total * lax.rsqrt(square / FF2 + norm_eps)).astype(bf16).astype(f32)
        mixed = resid_s[p, :, pl.ds(half, 1024)] + expert_sum[p * 8:(p + 1) * 8] + branch[p] * dense
        out_ref[p] = mixed.astype(bf16)

    for cp in sems.sent:
        cp.wait_send()
    pltpu.make_async_copy(
        meta_all.at[pl.ds(0, 63)], meta_all.at[pl.ds(0, 63)], meta_sems.at[0]
    ).wait()
    pltpu.make_async_copy(back.at[pl.ds(0, 63)], back.at[pl.ds(0, 63)], back_sems.at[0]).wait()


def layer_tail(partial, tokens, post_gain, branch_gate, meta, comb, dg, du, dd, eg, eu, ed):
    V = pltpu.VMEM
    vm = pl.BlockSpec(memory_space=pltpu.VMEM)
    hbm = pl.BlockSpec(memory_space=pl.ANY)
    scratch = [
        V((3, 8, 2048), bf16),
        V((3, 8, 2048), f32),
        V((3, 8, 2048), bf16),
        V((3, 4, 8, 1024), bf16),
        V((2, 4, 384, 1024), bf16),
        V((4, 384, 256), bf16),
        V((2048, 256), bf16),
        V((256, 1024), bf16),
        V((2048, 512), bf16),
        V((2048, 512), bf16),
        V((512, 2048), bf16),
        V((64, 1, 128), f32),
        V((64, 128), f32),
        V((2, 128, 1024), f32),
        V((4, 384, 1024), bf16),
        V((3, 2, 64, 1024), bf16),
        V((3, 2, 64, 1024), bf16),
        V((3, 64, 1024), bf16),
        V((3, 64, 1024), bf16),
        V((3, 64, 1024), bf16),
        V((3, 64, 1024), bf16),
        V((3, 4, 32, 1024), bf16),
        V((3, 3, 32, 1024), bf16),
        V((3, 4, 8, 1024), bf16),
        V((3, 3, 8, 1024), bf16),
        V((4, 3, 1, 128), f32),
        V((3, 3, 1, 128), f32),
        V((3, 4, 1, 128), f32),
        V((3, 3, 1, 128), f32),
        V((3, 4, 1, 128), f32),
        V((3, 3, 1, 128), f32),
        V((128, 1024), bf16),
        V((128, 1024), bf16),
        V((1024, 128), f32),
        V((64, 16, 128), bf16),
        V((64, 16, 128), bf16),
        pltpu.SemaphoreType.DMA((128,)),
        pltpu.SemaphoreType.DMA((128,)),
        pltpu.SemaphoreType.DMA((6,)),
        pltpu.SemaphoreType.DMA((2,)),
        pltpu.SemaphoreType.DMA((2,)),
    ]
    return pl.pallas_call(
        layer_kernel,
        out_shape=jax.ShapeDtypeStruct((3, 8, 1024), bf16),
        in_specs=[vm] * 6 + [hbm] * 6,
        out_specs=vm,
        scratch_shapes=scratch,
        compiler_params=pltpu.CompilerParams(
            collective_id=0, has_side_effects=True, vmem_limit_bytes=56 * 1024 * 1024
        ),
    )(partial, tokens, post_gain, branch_gate, meta, comb, dg, du, dd, eg, eu, ed)


def rms_scale(values, gain_vec):
    mean_square = jnp.mean(values * values, axis=-1, keepdims=True)
    return values * lax.rsqrt(mean_square + norm_eps) * gain_vec


def body(
    tokens,
    norm_gain,
    query_w,
    key_w,
    value_w,
    forget_w,
    forget_bias,
    query_gain,
    key_gain,
    cache_key,
    cache_value,
    cache_gate,
    cache_len,
    out_w,
    post_gain,
    branch_gate,
    dense_gate_w,
    dense_up_w,
    dense_down_w,
    expert_choice,
    route_weight,
    expert_gate_w,
    expert_up_w,
    expert_down_w,
):
    seq_count = tokens.shape[0]
    model_width = tokens.shape[1]
    heads_local = cache_gate.shape[1]
    kv_local = cache_key.shape[1]
    head_size = cache_key.shape[2]
    cache_span = cache_key.shape[3]
    ep_count = lax.axis_size("ep")
    tp_rank = lax.axis_index("tp")
    score_scale = head_size ** (-0.5)
    resid_in = tokens.astype(jnp.float32)
    normed = rms_scale(resid_in, norm_gain.astype(jnp.float32)).astype(jnp.bfloat16)
    queries = jnp.dot(normed, query_w, preferred_element_type=jnp.float32).reshape(
        seq_count, heads_local, head_size
    )
    queries = rms_scale(queries, query_gain.astype(jnp.float32)).astype(jnp.bfloat16)
    keys_all = jnp.dot(normed, key_w, preferred_element_type=jnp.float32).reshape(
        seq_count, -1, head_size
    )
    keys_all = rms_scale(keys_all, key_gain.astype(jnp.float32)).astype(jnp.bfloat16)
    values_all = (
        jnp.dot(normed, value_w, preferred_element_type=jnp.float32)
        .astype(jnp.bfloat16)
        .reshape(seq_count, -1, head_size)
    )
    fresh_key = lax.dynamic_slice_in_dim(keys_all, tp_rank * kv_local, kv_local, 1)
    fresh_value = lax.dynamic_slice_in_dim(values_all, tp_rank * kv_local, kv_local, 1)
    forget_all = jax.nn.log_sigmoid(
        jnp.dot(normed, forget_w, preferred_element_type=jnp.float32) + forget_bias
    )
    log_forget = lax.dynamic_slice_in_dim(forget_all, tp_rank * heads_local, heads_local, 1)
    repeat = heads_local // kv_local
    grouped = queries.reshape(seq_count, kv_local, repeat, head_size)
    scores = (
        jnp.einsum("sgrd,sgdl->sgrl", grouped, cache_key, preferred_element_type=jnp.float32)
        * score_scale
    )
    own_score = (
        jnp.einsum("sgrd,sgd->sgr", grouped, fresh_key, preferred_element_type=jnp.float32)
        * score_scale
    )
    current_slot_offset = lax.broadcasted_iota(jnp.int32, (seq_count, cache_span), 1)
    at_last = (current_slot_offset == cache_len[:, None] - 1)[:, None, :]
    previous = jnp.sum(jnp.where(at_last, cache_gate, jnp.zeros_like(cache_gate)), axis=2)
    current = previous + log_forget
    decay_bias = (current[:, :, None] - cache_gate).reshape(seq_count, kv_local, repeat, cache_span)
    is_valid = (current_slot_offset < cache_len[:, None])[:, None, None, :]
    logits = jnp.where(is_valid, scores + decay_bias, -jnp.inf)
    top_logit = jnp.maximum(jnp.max(logits, axis=3), own_score)
    weights = jnp.exp(logits - top_logit[..., None])
    own_weight = jnp.exp(own_score - top_logit)
    total_weight = jnp.sum(weights, axis=3) + own_weight
    cache_probs = (weights / total_weight[..., None]).astype(jnp.bfloat16)
    own_prob = (own_weight / total_weight).astype(jnp.bfloat16)
    mixed_heads = jnp.einsum(
        "sgrl,sgdl->sgrd", cache_probs, cache_value, preferred_element_type=jnp.float32
    )
    mixed_heads = (
        mixed_heads
        + own_prob.astype(jnp.float32)[..., None] * fresh_value.astype(jnp.float32)[:, :, None, :]
    )
    attn_heads = mixed_heads.reshape(seq_count, heads_local * head_size).astype(jnp.bfloat16)
    partial_value = jnp.dot(attn_heads, out_w, preferred_element_type=jnp.float32)
    capacity = 2
    route_ids = expert_choice.reshape(-1)
    member = (route_ids[:, None] == jnp.arange(ep_count)[None, :]).astype(jnp.int32)
    slot_index = jnp.sum((jnp.cumsum(member, axis=0) - member) * member, axis=1)
    target = route_ids * capacity + slot_index
    meta = jnp.pad(target.astype(jnp.float32), (0, 128 - target.shape[0]), constant_values=-1.0)
    target = target.reshape(seq_count, 2)
    places = jnp.arange(ep_count)[None, None, :] * 2 + jnp.arange(2)[:, None, None]
    comb = jnp.sum(
        jnp.where(target.T[:, None, :, None] == places[None], route_weight.T[:, None, :, None], 0.0),
        axis=0,
    )
    mixed = layer_tail(
        partial_value.astype(jnp.bfloat16).reshape(3, 8, model_width),
        tokens.reshape(3, 8, model_width),
        post_gain[None, :],
        branch_gate[None, :],
        meta[None, :],
        comb,
        dense_gate_w,
        dense_up_w,
        dense_down_w,
        expert_gate_w[0],
        expert_up_w[0],
        expert_down_w[0],
    )
    return (mixed.reshape(seq_count, 1024), fresh_key, fresh_value, current)


def solution(mesh):
    placed = (
        P("ep", None),
        P(),
        P(None, "tp"),
        P(),
        P(),
        P(),
        P(),
        P(),
        P(),
        P("ep", "tp", None, None),
        P("ep", "tp", None, None),
        P("ep", "tp", None),
        P("ep"),
        P("tp", None),
        P(),
        P(),
        P(None, ("ep", "tp")),
        P(None, ("ep", "tp")),
        P(("ep", "tp"), None),
        P("ep", None),
        P("ep", None),
        P("ep", None, "tp"),
        P("ep", None, "tp"),
        P("ep", "tp", None),
    )
    return jax.shard_map(
        body,
        mesh=mesh,
        in_specs=placed,
        out_specs=(P("ep", "tp"), P("ep", "tp", None), P("ep", "tp", None), P("ep", "tp")),
        check_vma=False,
    )
```

time: 241 us -> 90.8 us (0.38)
  starting transfers between devices: 63.8 us -> 0 us
  Pallas kernels: 0 us -> 63.7 us
  waiting for transfers between devices: 48.9 us -> 0 us
  local copies, waits for them, and re-layouts: 35.5 us -> 4.2 us
  other arithmetic: 31.9 us -> 8.13 us
  matrix products: 32.2 us -> 13.4 us
  between operations: 14.6 us -> 0.92 us
  blocking collectives: 12.1 us -> 0 us
    all_to_all x10 -> x0, starting transfers between devices: 63.8 us -> none  [the longest x2 22.1 us: moved(): lax.all_to_all(group, axis, split_axis=split_dim, concat_axis=concat_dim,...]
    pallas_call x0 -> x1, Pallas kernels: none -> 63.7 us  [layer_tail(): pl.pallas_call(layer_kernel, out_shape=jax.ShapeDtypeStruct((3, 8, 1024),...]
    all_to_all x10 -> x0, waiting for transfers between devices: 48.9 us -> none  [the longest x3 43.7 us: summed_on_arrival(): parts = lax.all_to_all(cut_along(array, dim, size), axis, 0, 0, tiled=True)]
    dot_general x10 -> x0, matrix products: 22.2 us -> none  [the longest x2 6.66 us: expert_work(): jnp.dot(activated, expert_down_w[0], preferred_element_type=jnp.float32)]
    all_to_all x2 -> x0, blocking collectives: 12.1 us -> none  [the longest x1 6.08 us: body(): lax.all_to_all(dense_up_w, 'tp', split_axis=0, concat_axis=1, tiled=True)]
    reduce_sum x8 -> x1, other arithmetic: 9.8 us -> 0.7 us  [body(): jnp.sum(jnp.where(target.T[:, None, :, None] == places[None], route_weigh...]
    reshape x6 -> x1, local copies, waits for them, and re-layouts: 8.41 us -> 0.1 us  [body(): route_ids = expert_choice.reshape(-1)]
    unnamed x53 -> x24, local copies, waits for them, and re-layouts: 9.71 us -> 1.57 us
  transfers between devices with their start and end apart: 11 -> 0, of which waited for: 5 -> 0; matrix products, arithmetic and copies ran while one was open for 29% -> 0% of each run, Pallas kernels for 0% -> 0%
where the time goes in v1:
time: 90.8 us; the launch traced here: 90.3 us
  Pallas kernels  63.7 us (70%)
  matrix products  13.4 us (15%)
  other arithmetic  8.13 us (9%)
  local copies, waits for them, and re-layouts  4.2 us (5%)
  between operations  0.92 us (1%)
    pallas_call x1, Pallas kernels, layer_tail(): pl.pallas_call(layer_kernel, out_shape=jax.ShapeDtypeStruct((3, 8, 1024),...  63.7 us
    dot_general x1, matrix products, body(): jnp.einsum('sgrl,sgdl->sgrd', cache_probs, cache_value, preferred_element...  3.11 us
    dot_general x1, matrix products, body(): jnp.einsum('sgrd,sgdl->sgrl', grouped, cache_key, preferred_element_type=...  2.66 us
    dot_general x1, matrix products, body(): jnp.dot(attn_heads, out_w, preferred_element_type=jnp.float32)  2.61 us
    dot_general x1, matrix products, body(): jnp.dot(normed, query_w, preferred_element_type=jnp.float32)  2.07 us

profile of v1, /device:TPU:0, one launch (start us, length us, event | category | flops | bytes accessed | tf_op | source)
XLA Modules:
  0.0 90.3 jit_solution(14545583152403222602)
XLA Ops:
  0.7 0.8 broadcast_add_fusion
  1.5 0.1 iota_compare_fusion
  1.6 1.4 %select_reduce_fusion = f32[24,8]{1,0:T(8,128)S(1)} fusion(f32[24,8,1024]{2,1,0:T(8,128)} %param.35, pred[24,1024]{1,0:T(8,128)(4,1)S(1)} %iota_compare_fusion), kind=kLoop, calls=%fused_computation.16 | loop fusion | flops 393024 | bytes 811776 | tf_op jit(solution)/shard_map/reduce_sum | solution.py:526
  3.0 0.7 convert_element_type.56
  3.7 1.0 %fusion.24 = f32[24]{0:T(128)S(1)} fusion(bf16[24,2048]{1,0:T(8,128)(2,1)} %param.24), kind=kLoop, calls=%fused_computation.22 | loop fusion | flops 147432 | bytes 98400 | tf_op jit(solution)/shard_map/reduce_sum | solution.py:454
  4.7 1.2 %fusion.45 = (f32[24,16]{0,1:T(8,128)S(1)}, f32[24,16]{0,1:T(8,128)S(1)}) fusion(f32[16]{0:T(128)} %param.30, bf16[2048,16]{0,1:T(8,128)(2,1)} %param.29, bf16[24,2048]{1,0:T(8,128)(2,1)} %param.24, f32[2048]{0:T(1024)S(1)} %convert_element_type.56, f32[24]{0:T(128)S(1)} %add_rsqrt_fusion.2), kind=kOutput, calls=%fused_computation.66 | convolution fusion | flops 1770624 | bytes 175264 | tf_op jit(solution)/shard_map/dot_general | solution.py:511
  6.0 2.1 %fusion.43 = f32[24,512]{1,0:T(8,128)S(1)} fusion(bf16[2048,512]{1,0:T(8,128)(2,1)} %param.26, bf16[24,2048]{1,0:T(8,128)(2,1)} %param.24, f32[2048]{0:T(1024)S(1)} %convert_element_type.56, f32[24]{0:T(128)S(1)} %add_rsqrt_fusion.2), kind=kOutput, calls=%fused_computation.65 | convolution fusion | flops 50528256 | bytes 2252896 | tf_op jit(solution)/shard_map/dot_general | solution.py:495
  8.1 0.1 reshape.190
  8.2 0.1 multiply_reduce_fusion
  8.3 0.1 iota_compare_fusion.1
  8.5 2.7 %fusion.46 = (f32[24,8]{1,0:T(8,128)S(1)}, f32[24,8,1024]{2,1,0:T(8,128)}) fusion(f32[24,8,1024]{2,1,0:T(8,128)} %param.35, f32[24,8]{1,0:T(8,128)S(1)} %copy.61, bf16[24,1,64,1024]{3,2,1,0:T(8,128)(2,1)S(1)} %copy-done, f32[24,8,64]{2,1,0:T(8,128)S(1)} %reshape.190, f32[64]{0:T(128)S(1)} %convert_element_type.58, f32[24,8]{1,0:T(8,128)S(1)} %add_rsqrt_fusion, ...), kind=kOutput, calls=%fused_computation.67 | convolution fusion | flops 26185536 | bytes 4794880 | tf_op jit(solution)/shard_map/sgrd,sgdl->sgrl/dot_general | solution.py:517
  11.2 0.2 fusion.40
  11.4 0.1 reshape.192
  11.5 0.1 multiply_reduce_fusion.1
  11.8 0.2 fusion.30
  12.1 1.4 %fusion.21 = f32[24,8]{1,0:T(8,128)S(1)} fusion(f32[24,8,1024]{2,1,0:T(8,128)} %get-tuple-element.11, f32[24,8]{1,0:T(8,128)S(1)} %multiply_maximum_fusion), kind=kLoop, calls=%fused_computation.17 | loop fusion | flops 393024 | bytes 787968 | tf_op jit(solution)/shard_map/reduce_sum | solution.py:534
  13.5 1.3 %convolution_convert_fusion.1 = bf16[24,128]{1,0:T(8,128)(2,1)S(1)} fusion(bf16[2048,128]{1,0:T(8,128)(2,1)} %param.28, bf16[24,2048]{1,0:T(8,128)(2,1)S(1)} %copy-done.1, f32[2048]{0:T(1024)S(1)} %convert_element_type.56, f32[24]{0:T(128)S(1)} %add_rsqrt_fusion.2), kind=kOutput, calls=%fused_computation.11 | convolution fusion | flops 12782592 | bytes 637024 | tf_op jit(solution)/shard_map/dot_general | solution.py:504
  14.9 0.6 bitcast_convert_fusion
  15.5 3.1 %fusion.17 = bf16[24,8,64]{2,1,0:T(8,128)(2,1)S(1)} fusion(bf16[24,1,64,1024]{3,2,1,0:T(8,128)(2,1)} %param.34, f32[24,8,1024]{2,1,0:T(8,128)} %get-tuple-element.11, f32[24,8]{1,0:T(8,128)S(1)} %get-tuple-element.7, f32[24,8]{1,0:T(8,128)S(1)} %multiply_maximum_fusion, f32[24,64]{1,0:T(8,128)S(1)} %get-tuple-element.4, f32[24,8]{1,0:T(8,128)S(1)} %get-tuple-element.6), kind=kOutput, calls=%fused_computation.10 | convolution fusion | flops 25792512 | bytes 3965184 | tf_op jit(solution)/shard_map/sgrl,sgdl->sgrd/dot_general | solution.py:537
  18.6 0.1 convert_element_type.67
  18.7 2.6 %fusion.4.partial_ref = bf16[3,8,2048]{2,1,0:T(8,128)(2,1)} fusion(bf16[24,512]{1,0:T(8,128)(2,1)S(1)} %convert_element_type.67, bf16[512,2048]{1,0:T(8,128)(2,1)} %param.37), kind=kOutput, calls=%fused_computation.5 | convolution fusion | flops 50380800 | bytes 2220032 | tf_op jit(solution)/shard_map/dot_general | solution.py:545
  21.4 0.6 broadcast_in_dim.40.gain_ref
  22.0 0.6 broadcast_in_dim.45.bgate_ref
  22.6 0.1 copy.65
  22.6 0.1 reshape.198
  22.9 0.2 select_reduce_fusion.2
  23.1 0.5 pad_bitcast_fusion.meta_ref
  23.6 0.1 reduce_sum.71
  23.8 0.7 select_reduce_fusion.1.comb_ref
  24.5 63.7 %shard_map.255 = bf16[3,8,1024]{2,1,0:T(8,128)(2,1)} custom-call(bf16[3,8,2048]{2,1,0:T(8,128)(2,1)} %fusion.4.partial_ref, bf16[3,8,2048]{2,1,0:T(8,128)(2,1)} %bitcast.44, bf16[1,2048]{1,0:T(2,128)(2,1)} %broadcast_in_dim.40.gain_ref, bf16[1,2048]{1,0:T(2,128)(2,1)} %broadcast_in_dim.45.bgate_ref, f32[1,128]{1,0:T(1,128)} %pad_bitcast_fusion.meta_ref, ...), custom_call_target="tpu_custom_call" | custom-call | tf_op jit(solution)/shard_map/pallas_call | solution.py:441
  88.2 0.7 fusion.29
  88.9 1.4 %copy.82 = bf16[24,1024]{1,0:T(8,128)(2,1)} copy(bf16[24,1024]{1,0:T(8,128)(2,1)} %bitcast.48) | data formatting | bytes 98304
  (45 shorter events, 0.8 us)
Async XLA Ops:
  0.6 7.8 %copy-start = (bf16[24,1,64,1024]{3,2,1,0:T(8,128)(2,1)S(1)}, bf16[24,1,64,1024]{3,2,1,0:T(8,128)(2,1)}, u32[]{:S(2)}) copy-start(bf16[24,1,64,1024]{3,2,1,0:T(8,128)(2,1)} %param.33) | copy-start | bytes 9437188
  0.6 7.7 %copy-start.8 = (s32[24]{0:T(128)S(1)}, s32[24]{0:T(128)}, u32[]{:S(2)}) copy-start(s32[24]{0:T(128)} %param.36) | copy-start | bytes 292
  0.7 7.5 %copy-start.9 = (bf16[64]{0:T(256)(128)(2,1)S(1)}, bf16[64]{0:T(256)(128)(2,1)}, u32[]{:S(2)}) copy-start(bf16[64]{0:T(256)(128)(2,1)} %param.31) | copy-start | bytes 388
  5.9 5.2 %copy-start.3 = (f32[24,8]{0,1:T(8,128)}, f32[24,8]{0,1:T(8,128)S(1)}, u32[]{:S(2)}) copy-start(f32[24,8]{0,1:T(8,128)S(1)} %fusion.34) | copy-start | bytes 2308
  8.4 2.7 %copy-start.10 = (bf16[64]{0:T(256)(128)(2,1)S(1)}, bf16[64]{0:T(256)(128)(2,1)}, u32[]{:S(2)}) copy-start(bf16[64]{0:T(256)(128)(2,1)} %param.32) | copy-start | bytes 388
  8.5 2.7 %copy-start.1 = (bf16[24,2048]{1,0:T(8,128)(2,1)S(1)}, bf16[24,2048]{1,0:T(8,128)(2,1)}, u32[]{:S(2)}) copy-start(bf16[24,2048]{1,0:T(8,128)(2,1)} %param.24) | copy-start | bytes 294916
  8.5 2.7 %copy-start.2 = (bf16[2048,128]{1,0:T(8,128)(2,1)S(1)}, bf16[2048,128]{1,0:T(8,128)(2,1)}, u32[]{:S(2)}) copy-start(bf16[2048,128]{1,0:T(8,128)(2,1)} %param.27) | copy-start | bytes 1572868
  18.6 2.8 %copy-start.4 = (bf16[2048]{0:T(1024)(128)(2,1)S(1)}, bf16[2048]{0:T(1024)(128)(2,1)}, u32[]{:S(2)}) copy-start(bf16[2048]{0:T(1024)(128)(2,1)} %param.38) | copy-start | bytes 12292
  18.6 3.4 %copy-start.5 = (bf16[2048]{0:T(1024)(128)(2,1)S(1)}, bf16[2048]{0:T(1024)(128)(2,1)}, u32[]{:S(2)}) copy-start(bf16[2048]{0:T(1024)(128)(2,1)} %param.39) | copy-start | bytes 12292
  18.6 4.0 %copy-start.6 = (s32[24,2]{0,1:T(2,128)S(1)}, s32[24,2]{0,1:T(2,128)}, u32[]{:S(2)}) copy-start(s32[24,2]{0,1:T(2,128)} %param.43) | copy-start | bytes 580
  18.6 5.2 %copy-start.7 = (f32[24,2]{0,1:T(2,128)S(1)}, f32[24,2]{0,1:T(2,128)}, u32[]{:S(2)}) copy-start(f32[24,2]{0,1:T(2,128)} %param.44) | copy-start | bytes 580

commit v2 on v1

--- a/solution.py
+++ b/solution.py
@@ -40,13 +40,16 @@
 
 
 def layer_kernel(
-    partial_ref, tokens_ref, gain_ref, bgate_ref, meta_ref, comb_ref,
+    len_ref, tokens_h, ngain_h, pgain_h, bgate_h, qgain_h, kgain_h, fbias_h, choice_h, rweight_h,
+    qw_h, kw_h, vw_h, fw_h, kc_h, vc_h, cg_h, ow_h,
     dg_h, du_h, dd_h, eg_h, eu_h, ed_h,
-    out_ref,
-    partner_part, resid_s, pn_s, a1, xs, hid, wgu, wd, eg, eu, ed,
+    out_ref, fk_ref, fv_ref, fg_ref,
+    tok_s, ngain_s, pgain_s, bgate_s, qgain_s, kgain_s, fbias_s, choice_s, rweight_s,
+    qw, kw, vw, fw, kc, vc, cg, ow, rows_s, q_s, kf_s, vf_s, o_s, ah_s, meta_s, comb_s,
+    partial_s, partner_part, resid_s, pn_s, a1, xs, hid, wgu, wd, eg, eu, ed,
     meta_all, meta_tab, xg, dens, rl, rr, ql, qr, sl, sr, t2, r2, t3, r3,
     sq, sq1, sq2, sq2r, sq3, sq3r, ep_send, ep_recv, ret_f, ret_b, back,
-    send_sem, recv_sem, load_sem, meta_sems, back_sems,
+    send_sem, recv_sem, load_sem, small_sem, cache_sem, meta_sems, back_sems,
 ):
     me = lax.axis_index("ep")
     core = lax.axis_index("tp")
@@ -64,6 +67,35 @@
 
     sems = Sems(send_sem, recv_sem)
 
+    barrier = pltpu.get_barrier_semaphore()
+    pl.semaphore_signal(barrier, inc=1, device_id=partner, device_id_type=MESH)
+
+    @pl.loop(1, 64)
+    def _(i):
+        pl.semaphore_signal(
+            barrier, inc=1, device_id=((me + i) % 64, core), device_id_type=MESH
+        )
+
+    smalls = []
+    for i, (src, dst) in enumerate((
+        (tokens_h, tok_s), (ngain_h, ngain_s), (choice_h, choice_s), (rweight_h, rweight_s),
+        (qw_h, qw), (kw_h, kw), (vw_h, vw), (fw_h, fw), (fbias_h, fbias_s),
+        (qgain_h, qgain_s), (kgain_h, kgain_s), (pgain_h, pgain_s), (bgate_h, bgate_s),
+    )):
+        cp = pltpu.make_async_copy(src, dst, small_sem.at[i])
+        cp.start()
+        smalls.append(cp)
+
+    def cache_copies(g):
+        rows = pl.ds(g * 4, 4)
+        return [
+            pltpu.make_async_copy(src.at[rows], dst.at[rows], cache_sem.at[i, g])
+            for i, (src, dst) in enumerate(((kc_h, kc), (cg_h, cg), (vc_h, vc)))
+        ]
+
+    for g in range(6):
+        for cp in cache_copies(g):
+            cp.start()
     loads = []
     for i, (src, dst) in enumerate((
         (dg_h, wgu.at[:, pl.ds(0, 128)]),
@@ -72,28 +104,131 @@
         (eg_h, eg),
         (eu_h, eu),
         (ed_h, ed),
+        (ow_h, ow),
     )):
-        cp = pltpu.make_async_copy(src, dst, load_sem.at[i])
+        loads.append(pltpu.make_async_copy(src, dst, load_sem.at[i]))
+    loads[6].start()
+
+    def column(row):
+        pick = lax.broadcasted_iota(jnp.int32, (24, 24), 0) == lax.broadcasted_iota(jnp.int32, (24, 24), 1)
+        return jnp.sum(jnp.where(pick, row, jnp.zeros_like(row)), axis=1, keepdims=True)
+
+    smalls[2].wait()
+    smalls[3].wait()
+    choice = choice_s[...].astype(f32)
+    named = [choice[k:k + 1, :] for k in range(2)]
+    named_col = [column(v) for v in named]
+    earlier = lax.broadcasted_iota(jnp.int32, (24, 24), 0) < lax.broadcasted_iota(jnp.int32, (24, 24), 1)
+    targets = []
+    for k in range(2):
+        again = jnp.zeros((1, 24), f32)
+        for i in range(2):
+            same = jnp.where(earlier & (named_col[i] == named[k]), 1.0, 0.0)
+            again = again + jnp.sum(same, axis=0, keepdims=True)
+        targets.append(named[k] * 2.0 + jnp.minimum(again, 1.0))
+    meta_s[...] = jnp.full((1, 128), -1.0, f32)
+    meta_s[:, pl.ds(0, 24)] = targets[0] + 128.0 * targets[1]
+    target_col = [column(v) for v in targets]
+    weight_col = [column(rweight_s[k:k + 1, :]) for k in range(2)]
+    place = lax.broadcasted_iota(jnp.int32, (24, 64), 1).astype(f32) * 2.0
+    for t in range(2):
+        m = jnp.where(target_col[0] == place + t, weight_col[0], 0.0)
+        comb_s[t] = m + jnp.where(target_col[1] == place + t, weight_col[1], 0.0)
+
+    for i in (1, 11, 12):
+        smalls[i].wait()
+    for i, src in enumerate((ngain_s, pgain_s, bgate_s)):
+        v = src[...].astype(f32)
+        for t in range(16):
+            rows_s[pl.ds(i, 1), pl.ds(t * 128, 128)] = v[t:t + 1]
+    smalls[0].wait()
+    toks = tok_s[...].astype(f32)
+    mean_square = jnp.mean(toks * toks, axis=-1, keepdims=True)
+    normed = (toks * lax.rsqrt(mean_square + norm_eps) * rows_s[pl.ds(0, 1), :]).astype(bf16)
+
+    def head_norm(v, gain):
+        return v * lax.rsqrt(jnp.mean(v * v, axis=-1, keepdims=True) + norm_eps) * gain
+
+    smalls[4].wait()
+    q_all = jnp.dot(normed, qw[...], preferred_element_type=f32)
+    smalls[9].wait()
+    qg = qgain_s[...].astype(f32)
+    for h in range(8):
+        q = head_norm(q_all[:, h * 64:(h + 1) * 64], qg).astype(bf16).astype(f32)
+        q_s[pl.ds(h, 24, stride=8), :] = jnp.concatenate([q, jnp.zeros_like(q)], axis=1)
+    smalls[5].wait()
+    smalls[10].wait()
+    k_all = jnp.dot(normed, kw[...], preferred_element_type=f32)
+    k_own = head_norm(jnp.where(core == 0, k_all[:, :64], k_all[:, 64:]), kgain_s[...].astype(f32))
+    fk_ref[...] = k_own.astype(bf16)
+    kf_s[...] = k_own.astype(bf16).astype(f32)
+    smalls[6].wait()
+    v_all = jnp.dot(normed, vw[...], preferred_element_type=f32)
+    v_own = jnp.where(core == 0, v_all[:, :64], v_all[:, 64:]).astype(bf16)
+    fv_ref[...] = v_own
+    vf_s[...] = v_own.astype(f32)
+    smalls[7].wait()
+    smalls[8].wait()
+    forget = lax.dot_general(
+        fw[...], normed, (((1,), (1,)), ((), ())), preferred_element_type=f32
+    )
+    pick16 = lax.broadcasted_iota(jnp.int32, (16, 16), 0) == lax.broadcasted_iota(jnp.int32, (16, 16), 1)
+    forget = forget + jnp.sum(jnp.where(pick16, fbias_s[...], 0.0), axis=1, keepdims=True)
+    log_forget = jnp.minimum(forget, 0.0) - jnp.log1p(jnp.exp(-jnp.abs(forget)))
+    log_forget = jnp.where(core == 0, log_forget[:8], log_forget[8:])
+
+    slot_at = lax.broadcasted_iota(jnp.int32, (8, 1024), 1)
+    seq_lane = lax.broadcasted_iota(jnp.int32, (8, 24), 1)
+    scale = 64 ** (-0.5)
+
+    def attend(g, gates):
+        for cp in cache_copies(g):
+            cp.wait()
+        for i in range(4):
+            s = g * 4 + i
+            rows = pl.ds(pl.multiple_of(s * 8, 8), 8)
+            length = len_ref[s]
+            q = q_s[rows, :][:, :64]
+            score = jnp.dot(q.astype(bf16), kc[s], preferred_element_type=f32) * scale
+            gate = cg[s]
+            current = jnp.sum(jnp.where(slot_at == length - 1, gate, 0.0), axis=1, keepdims=True)
+            current = current + jnp.sum(
+                jnp.where(seq_lane == s, log_forget, 0.0), axis=1, keepdims=True
+            )
+            gates = jnp.where(seq_lane == s, current, gates)
+            own = jnp.sum(q * kf_s[pl.ds(s, 1), :], axis=1, keepdims=True) * scale
+            logit = jnp.where(slot_at < length, score + (current - gate), -jnp.inf)
+            top = jnp.maximum(jnp.max(logit, axis=1, keepdims=True), own)
+            w = jnp.exp(logit - top)
+            own_w = jnp.exp(own - top)
+            inv = 1.0 / (jnp.sum(w, axis=1, keepdims=True) + own_w)
+            probs = (w * inv).astype(bf16)
+            own_p = (own_w * inv).astype(bf16).astype(f32)
+            o = lax.dot_general(
+                probs, vc[s], (((1,), (1,)), ((), ())), preferred_element_type=f32
+            )
+            o = o + own_p * vf_s[pl.ds(s, 1), :]
+            o_s[rows, :] = jnp.concatenate([o, jnp.zeros_like(o)], axis=1)
+        return gates
+
+    gates = lax.fori_loop(0, 6, attend, jnp.zeros((8, 24), f32))
+    fg_ref[...] = gates
+    for cp in loads[:6]:
         cp.start()
-        loads.append(cp)
-
-    barrier = pltpu.get_barrier_semaphore()
-    pl.semaphore_signal(barrier, inc=1, device_id=partner, device_id_type=MESH)
-
-    @pl.loop(1, 64)
-    def _(i):
-        pl.semaphore_signal(
-            barrier, inc=1, device_id=((me + i) % 64, core), device_id_type=MESH
-        )
+    for h in range(8):
+        ah_s[:, pl.ds(h * 64, 64)] = o_s[pl.ds(h, 24, stride=8), :][:, :64]
+    loads[6].wait()
+    partial = jnp.dot(ah_s[...].astype(bf16), ow[...], preferred_element_type=f32)
+    partial_s[...] = partial.reshape(3, 8, 2048).astype(bf16)
 
     pl.semaphore_wait(barrier, 64)
 
-    part_cp = sems.copy(partial_ref, partner_part, partner)
+    part_cp = sems.copy(partial_s, partner_part, partner)
     wd_cp = sems.copy(dd_h.at[:, pl.ds(ohalf, 1024)], wd.at[pl.ds(ccol, 128)], partner)
 
     def meta_copy(d):
         return pltpu.make_async_remote_copy(
-            src_ref=meta_ref,
+            src_ref=meta_s,
             dst_ref=meta_all.at[me],
             send_sem=meta_sems.at[0],
             recv_sem=meta_sems.at[1],
@@ -102,11 +237,11 @@
         )
 
     part_cp.wait_recv()
-    attn = partial_ref[...].astype(f32) + partner_part[...].astype(f32)
-    resid = (tokens_ref[...].astype(f32) + attn).astype(bf16).astype(f32)
+    attn = partial_s[...].astype(f32) + partner_part[...].astype(f32)
+    resid = (tok_s[...].astype(f32).reshape(3, 8, 2048) + attn).astype(bf16).astype(f32)
     resid_s[...] = resid
     mean_square = jnp.mean(resid * resid, axis=-1, keepdims=True)
-    gain = gain_ref[...].astype(f32)[None]
+    gain = rows_s[pl.ds(1, 1), :][None]
     post = (resid * lax.rsqrt(mean_square + norm_eps) * gain).astype(bf16)
     pn_s[...] = post
     a1[:, 0] = pn_s[:, :, pl.ds(half, 1024)]
@@ -120,9 +255,9 @@
     def _(i):
         meta_copy((me + i) % 64).start()
 
-    meta_all[me] = meta_ref[...]
+    meta_all[me] = meta_s[...]
     branch = jax.nn.sigmoid(
-        jnp.sum(post.astype(f32) * bgate_ref[...].astype(f32)[None], axis=-1, keepdims=True)
+        jnp.sum(post.astype(f32) * rows_s[pl.ds(2, 1), :][None], axis=-1, keepdims=True)
     )
 
     g2 = []
@@ -162,7 +297,7 @@
     ).wait()
     for d in range(64):
         meta_tab[pl.ds(d, 1), :] = meta_all[d]
-    table = meta_tab[...]
+    table = meta_tab[...].astype(jnp.int32)
     lane = lax.broadcasted_iota(jnp.int32, (64, 128), 1)
     dev = lax.broadcasted_iota(jnp.int32, (64, 1), 0)
     shift = [((dev >> s) - coords[i]) & 3 for i, s in enumerate((0, 2, 4))]
@@ -173,8 +308,9 @@
         starts.append(slot * 384 + p * 128 + kb * 32 + ka * 8)
     row_ids = []
     for s in range(2):
-        want = (me * 2 + s).astype(f32)
-        tok = jnp.sum(jnp.where(table == want, (lane >> 1) + 1, 0), axis=1, keepdims=True) - 1
+        want = me * 2 + s
+        hit = (lane < 24) & (((table & 127) == want) | ((table >> 7) == want))
+        tok = jnp.sum(jnp.where(hit, lane + 1, 0), axis=1, keepdims=True) - 1
         start = jnp.where(tok < 8, starts[0], jnp.where(tok < 16, starts[1], starts[2]))
         row_ids.append(jnp.where(tok < 0, -1, start + (tok & 7)))
     row_id = jnp.concatenate(row_ids, axis=0)
@@ -344,7 +480,7 @@
         m = 0.0
         for s in range(2):
             m = m + jnp.dot(
-                comb_ref[s], ret_f[pl.ds(s * 8 + t, 64, stride=16), :],
+                comb_s[s], ret_f[pl.ds(s * 8 + t, 64, stride=16), :],
                 preferred_element_type=f32, precision=lax.Precision.HIGHEST,
             )
         mixes.append(m)
@@ -391,11 +527,37 @@
     pltpu.make_async_copy(back.at[pl.ds(0, 63)], back.at[pl.ds(0, 63)], back_sems.at[0]).wait()
 
 
-def layer_tail(partial, tokens, post_gain, branch_gate, meta, comb, dg, du, dd, eg, eu, ed):
+def fused_layer(lens, *args):
     V = pltpu.VMEM
     vm = pl.BlockSpec(memory_space=pltpu.VMEM)
     hbm = pl.BlockSpec(memory_space=pl.ANY)
     scratch = [
+        V((24, 2048), bf16),
+        V((16, 128), bf16),
+        V((16, 128), bf16),
+        V((16, 128), bf16),
+        V((1, 64), bf16),
+        V((1, 64), bf16),
+        V((1, 16), f32),
+        V((2, 24), jnp.int32),
+        V((2, 24), f32),
+        V((2048, 512), bf16),
+        V((2048, 128), bf16),
+        V((2048, 128), bf16),
+        V((16, 2048), bf16),
+        V((24, 64, 1024), bf16),
+        V((24, 64, 1024), bf16),
+        V((24, 8, 1024), f32),
+        V((512, 2048), bf16),
+        V((8, 2048), f32),
+        V((192, 128), f32),
+        V((24, 64), f32),
+        V((24, 64), f32),
+        V((192, 128), f32),
+        V((24, 512), f32),
+        V((1, 128), f32),
+        V((2, 24, 64), f32),
+        V((3, 8, 2048), bf16),
         V((3, 8, 2048), bf16),
         V((3, 8, 2048), f32),
         V((3, 8, 2048), bf16),
@@ -434,25 +596,27 @@
         V((64, 16, 128), bf16),
         pltpu.SemaphoreType.DMA((128,)),
         pltpu.SemaphoreType.DMA((128,)),
-        pltpu.SemaphoreType.DMA((6,)),
+        pltpu.SemaphoreType.DMA((7,)),
+        pltpu.SemaphoreType.DMA((13,)),
+        pltpu.SemaphoreType.DMA((3, 6)),
         pltpu.SemaphoreType.DMA((2,)),
         pltpu.SemaphoreType.DMA((2,)),
     ]
     return pl.pallas_call(
         layer_kernel,
-        out_shape=jax.ShapeDtypeStruct((3, 8, 1024), bf16),
-        in_specs=[vm] * 6 + [hbm] * 6,
-        out_specs=vm,
+        out_shape=(
+            jax.ShapeDtypeStruct((3, 8, 1024), bf16),
+            jax.ShapeDtypeStruct((24, 64), bf16),
+            jax.ShapeDtypeStruct((24, 64), bf16),
+            jax.ShapeDtypeStruct((8, 24), f32),
+        ),
+        in_specs=[pl.BlockSpec(memory_space=pltpu.SMEM)] + [hbm] * len(args),
+        out_specs=(vm,) * 4,
         scratch_shapes=scratch,
         compiler_params=pltpu.CompilerParams(
             collective_id=0, has_side_effects=True, vmem_limit_bytes=56 * 1024 * 1024
         ),
-    )(partial, tokens, post_gain, branch_gate, meta, comb, dg, du, dd, eg, eu, ed)
-
-
-def rms_scale(values, gain_vec):
-    mean_square = jnp.mean(values * values, axis=-1, keepdims=True)
-    return values * lax.rsqrt(mean_square + norm_eps) * gain_vec
+    )(lens, *args)
 
 
 def body(
@@ -481,95 +645,38 @@
     expert_up_w,
     expert_down_w,
 ):
-    seq_count = tokens.shape[0]
-    model_width = tokens.shape[1]
-    heads_local = cache_gate.shape[1]
-    kv_local = cache_key.shape[1]
-    head_size = cache_key.shape[2]
-    cache_span = cache_key.shape[3]
-    ep_count = lax.axis_size("ep")
-    tp_rank = lax.axis_index("tp")
-    score_scale = head_size ** (-0.5)
-    resid_in = tokens.astype(jnp.float32)
-    normed = rms_scale(resid_in, norm_gain.astype(jnp.float32)).astype(jnp.bfloat16)
-    queries = jnp.dot(normed, query_w, preferred_element_type=jnp.float32).reshape(
-        seq_count, heads_local, head_size
-    )
-    queries = rms_scale(queries, query_gain.astype(jnp.float32)).astype(jnp.bfloat16)
-    keys_all = jnp.dot(normed, key_w, preferred_element_type=jnp.float32).reshape(
-        seq_count, -1, head_size
-    )
-    keys_all = rms_scale(keys_all, key_gain.astype(jnp.float32)).astype(jnp.bfloat16)
-    values_all = (
-        jnp.dot(normed, value_w, preferred_element_type=jnp.float32)
-        .astype(jnp.bfloat16)
-        .reshape(seq_count, -1, head_size)
-    )
-    fresh_key = lax.dynamic_slice_in_dim(keys_all, tp_rank * kv_local, kv_local, 1)
-    fresh_value = lax.dynamic_slice_in_dim(values_all, tp_rank * kv_local, kv_local, 1)
-    forget_all = jax.nn.log_sigmoid(
-        jnp.dot(normed, forget_w, preferred_element_type=jnp.float32) + forget_bias
-    )
-    log_forget = lax.dynamic_slice_in_dim(forget_all, tp_rank * heads_local, heads_local, 1)
-    repeat = heads_local // kv_local
-    grouped = queries.reshape(seq_count, kv_local, repeat, head_size)
-    scores = (
-        jnp.einsum("sgrd,sgdl->sgrl", grouped, cache_key, preferred_element_type=jnp.float32)
-        * score_scale
-    )
-    own_score = (
-        jnp.einsum("sgrd,sgd->sgr", grouped, fresh_key, preferred_element_type=jnp.float32)
-        * score_scale
-    )
-    current_slot_offset = lax.broadcasted_iota(jnp.int32, (seq_count, cache_span), 1)
-    at_last = (current_slot_offset == cache_len[:, None] - 1)[:, None, :]
-    previous = jnp.sum(jnp.where(at_last, cache_gate, jnp.zeros_like(cache_gate)), axis=2)
-    current = previous + log_forget
-    decay_bias = (current[:, :, None] - cache_gate).reshape(seq_count, kv_local, repeat, cache_span)
-    is_valid = (current_slot_offset < cache_len[:, None])[:, None, None, :]
-    logits = jnp.where(is_valid, scores + decay_bias, -jnp.inf)
-    top_logit = jnp.maximum(jnp.max(logits, axis=3), own_score)
-    weights = jnp.exp(logits - top_logit[..., None])
-    own_weight = jnp.exp(own_score - top_logit)
-    total_weight = jnp.sum(weights, axis=3) + own_weight
-    cache_probs = (weights / total_weight[..., None]).astype(jnp.bfloat16)
-    own_prob = (own_weight / total_weight).astype(jnp.bfloat16)
-    mixed_heads = jnp.einsum(
-        "sgrl,sgdl->sgrd", cache_probs, cache_value, preferred_element_type=jnp.float32
-    )
-    mixed_heads = (
-        mixed_heads
-        + own_prob.astype(jnp.float32)[..., None] * fresh_value.astype(jnp.float32)[:, :, None, :]
-    )
-    attn_heads = mixed_heads.reshape(seq_count, heads_local * head_size).astype(jnp.bfloat16)
-    partial_value = jnp.dot(attn_heads, out_w, preferred_element_type=jnp.float32)
-    capacity = 2
-    route_ids = expert_choice.reshape(-1)
-    member = (route_ids[:, None] == jnp.arange(ep_count)[None, :]).astype(jnp.int32)
-    slot_index = jnp.sum((jnp.cumsum(member, axis=0) - member) * member, axis=1)
-    target = route_ids * capacity + slot_index
-    meta = jnp.pad(target.astype(jnp.float32), (0, 128 - target.shape[0]), constant_values=-1.0)
-    target = target.reshape(seq_count, 2)
-    places = jnp.arange(ep_count)[None, None, :] * 2 + jnp.arange(2)[:, None, None]
-    comb = jnp.sum(
-        jnp.where(target.T[:, None, :, None] == places[None], route_weight.T[:, None, :, None], 0.0),
-        axis=0,
-    )
-    mixed = layer_tail(
-        partial_value.astype(jnp.bfloat16).reshape(3, 8, model_width),
-        tokens.reshape(3, 8, model_width),
-        post_gain[None, :],
-        branch_gate[None, :],
-        meta[None, :],
-        comb,
+    mixed, fresh_key, fresh_value, fresh_gate = fused_layer(
+        cache_len,
+        tokens,
+        norm_gain.reshape(16, 128),
+        post_gain.reshape(16, 128),
+        branch_gate.reshape(16, 128),
+        query_gain.reshape(1, 64),
+        key_gain.reshape(1, 64),
+        forget_bias.reshape(1, 16),
+        expert_choice.T,
+        route_weight.T,
+        query_w,
+        key_w,
+        value_w,
+        forget_w.T,
+        cache_key.reshape(24, 64, 1024),
+        cache_value.reshape(24, 64, 1024),
+        cache_gate,
+        out_w,
         dense_gate_w,
         dense_up_w,
         dense_down_w,
-        expert_gate_w[0],
-        expert_up_w[0],
-        expert_down_w[0],
+        expert_gate_w.reshape(2048, 512),
+        expert_up_w.reshape(2048, 512),
+        expert_down_w.reshape(512, 2048),
     )
-    return (mixed.reshape(seq_count, 1024), fresh_key, fresh_value, current)
+    return (
+        mixed.reshape(24, 1024),
+        fresh_key.reshape(24, 1, 64),
+        fresh_value.reshape(24, 1, 64),
+        fresh_gate.T,
+    )
 
 
 def solution(mesh):

time: 90.8 us -> 77.9 us (0.86)
  matrix products: 13.4 us -> 0 us
  other arithmetic: 8.13 us -> 0 us
  Pallas kernels: 63.7 us -> 71.7 us
  local copies, waits for them, and re-layouts: 4.2 us -> 5.27 us
    dot_general x8 -> x0, matrix products: 13.4 us -> none  [the longest x1 3.11 us: body(): jnp.einsum('sgrl,sgdl->sgrd', cache_probs, cache_value, preferred_element...]
    pallas_call x1, Pallas kernels: 63.7 us -> 71.7 us  [fused_layer(): pl.pallas_call(layer_kernel, out_shape=(jax.ShapeDtypeStruct((3, 8, 1024)...]
    reduce_sum x7 -> x0, other arithmetic: 4.86 us -> none  [the longest x1 1.39 us: body(): total_weight = jnp.sum(weights, axis=3) + own_weight]
    unnamed x24 -> x4, local copies, waits for them, and re-layouts: 1.57 us -> 5.27 us
    broadcast_in_dim x3 -> x0, local copies, waits for them, and re-layouts: 1.72 us -> none  [the longest x1 0.6 us: body(): branch_gate[None, :]]
    convert_element_type x7 -> x0, other arithmetic: 1.46 us -> none  [the longest x1 0.69 us: body(): norm_gain.astype(jnp.float32)]
where the time goes in v2:
time: 77.9 us; the launch traced here: 77.6 us
  Pallas kernels  71.7 us (92%)
  local copies, waits for them, and re-layouts  5.27 us (7%)
    pallas_call x1, Pallas kernels, fused_layer(): pl.pallas_call(layer_kernel, out_shape=(jax.ShapeDtypeStruct((3, 8, 1024)...  71.7 us
    unnamed x4, local copies, waits for them, and re-layouts  5.27 us

profile of v2, /device:TPU:0, one launch (start us, length us, event | category | flops | bytes accessed | tf_op | source)
XLA Modules:
  0.0 77.6 jit_solution(1182356503862109440)
XLA Ops:
  0.6 71.7 %shard_map.255 = (bf16[3,8,1024]{2,1,0:T(8,128)(2,1)}, bf16[24,64]{1,0:T(8,128)(2,1)}, bf16[24,64]{1,0:T(8,128)(2,1)}, f32[8,24]{1,0:T(8,128)}) custom-call(s32[24]{0:T(128)} %len_ref.1, bf16[24,2048]{1,0:T(8,128)(2,1)} %tokens_h.1, bf16[16,128]{1,0:T(8,128)(2,1)} %bitcast.28, bf16[16,128]{1,0:T(8,128)(2,1)} %bitcast.29, bf16[16,128]{1,0:T(8,128)(2,1)} %bitcast.30, ...), custom_call_target="tpu_custom_call" | custom-call | tf_op jit(solution)/shard_map/pallas_call | solution.py:605
  72.4 1.4 %copy.32 = bf16[24,1024]{1,0:T(8,128)(2,1)} copy(bf16[24,1024]{1,0:T(8,128)(2,1)} %bitcast.24) | data formatting | bytes 98304
  73.8 1.3 %copy.33 = bf16[24,1,64]{2,0,1:T(8,128)(2,1)} copy(bf16[24,1,64]{2,0,1:T(8,128)(2,1)} %bitcast.26) | data formatting | bytes 6144
  75.1 1.3 %copy.34 = bf16[24,1,64]{2,0,1:T(8,128)(2,1)} copy(bf16[24,1,64]{2,0,1:T(8,128)(2,1)} %bitcast.25) | data formatting | bytes 6144
  76.4 1.3 %copy.35 = f32[24,8]{0,1:T(8,128)} copy(f32[24,8]{0,1:T(8,128)} %bitcast.27) | data formatting | bytes 1536

commit v3 on v2

--- a/solution.py
+++ b/solution.py
@@ -45,11 +45,11 @@
     dg_h, du_h, dd_h, eg_h, eu_h, ed_h,
     out_ref, fk_ref, fv_ref, fg_ref,
     tok_s, ngain_s, pgain_s, bgate_s, qgain_s, kgain_s, fbias_s, choice_s, rweight_s,
-    qw, kw, vw, fw, kc, vc, cg, ow, rows_s, q_s, kf_s, vf_s, o_s, ah_s, meta_s, comb_s,
+    qw, kw, vw, fw, kc, vc, cg, ow, rows_s, q_s, kf_s, vf_s, o_s, ah_s, comb_s,
     partial_s, partner_part, resid_s, pn_s, a1, xs, hid, wgu, wd, eg, eu, ed,
     meta_all, meta_tab, xg, dens, rl, rr, ql, qr, sl, sr, t2, r2, t3, r3,
     sq, sq1, sq2, sq2r, sq3, sq3r, ep_send, ep_recv, ret_f, ret_b, back,
-    send_sem, recv_sem, load_sem, small_sem, cache_sem, meta_sems, back_sems,
+    send_sem, recv_sem, load_sem, small_sem, cache_sem, back_sems,
 ):
     me = lax.axis_index("ep")
     core = lax.axis_index("tp")
@@ -70,11 +70,9 @@
     barrier = pltpu.get_barrier_semaphore()
     pl.semaphore_signal(barrier, inc=1, device_id=partner, device_id_type=MESH)
 
-    @pl.loop(1, 64)
-    def _(i):
-        pl.semaphore_signal(
-            barrier, inc=1, device_id=((me + i) % 64, core), device_id_type=MESH
-        )
+    for dim in range(3):
+        for k in (1, 2, 3):
+            pl.semaphore_signal(barrier, inc=1, device_id=peer(dim, k), device_id_type=MESH)
 
     smalls = []
     for i, (src, dst) in enumerate((
@@ -93,9 +91,6 @@
             for i, (src, dst) in enumerate(((kc_h, kc), (cg_h, cg), (vc_h, vc)))
         ]
 
-    for g in range(6):
-        for cp in cache_copies(g):
-            cp.start()
     loads = []
     for i, (src, dst) in enumerate((
         (dg_h, wgu.at[:, pl.ds(0, 128)]),
@@ -107,7 +102,7 @@
         (ow_h, ow),
     )):
         loads.append(pltpu.make_async_copy(src, dst, load_sem.at[i]))
-    loads[6].start()
+    meta_all[0] = jnp.full((1, 128), -1.0, f32)
 
     def column(row):
         pick = lax.broadcasted_iota(jnp.int32, (24, 24), 0) == lax.broadcasted_iota(jnp.int32, (24, 24), 1)
@@ -126,14 +121,19 @@
             same = jnp.where(earlier & (named_col[i] == named[k]), 1.0, 0.0)
             again = again + jnp.sum(same, axis=0, keepdims=True)
         targets.append(named[k] * 2.0 + jnp.minimum(again, 1.0))
-    meta_s[...] = jnp.full((1, 128), -1.0, f32)
-    meta_s[:, pl.ds(0, 24)] = targets[0] + 128.0 * targets[1]
+    meta_all[0, :, pl.ds(0, 24)] = targets[0] + 128.0 * targets[1]
     target_col = [column(v) for v in targets]
     weight_col = [column(rweight_s[k:k + 1, :]) for k in range(2)]
     place = lax.broadcasted_iota(jnp.int32, (24, 64), 1).astype(f32) * 2.0
     for t in range(2):
         m = jnp.where(target_col[0] == place + t, weight_col[0], 0.0)
         comb_s[t] = m + jnp.where(target_col[1] == place + t, weight_col[1], 0.0)
+
+    smalls[4].wait()
+    for g in range(6):
+        for cp in cache_copies(g):
+            cp.start()
+    loads[6].start()
 
     for i in (1, 11, 12):
         smalls[i].wait()
@@ -149,7 +149,6 @@
     def head_norm(v, gain):
         return v * lax.rsqrt(jnp.mean(v * v, axis=-1, keepdims=True) + norm_eps) * gain
 
-    smalls[4].wait()
     q_all = jnp.dot(normed, qw[...], preferred_element_type=f32)
     smalls[9].wait()
     qg = qgain_s[...].astype(f32)
@@ -221,20 +220,10 @@
     partial = jnp.dot(ah_s[...].astype(bf16), ow[...], preferred_element_type=f32)
     partial_s[...] = partial.reshape(3, 8, 2048).astype(bf16)
 
-    pl.semaphore_wait(barrier, 64)
+    pl.semaphore_wait(barrier, 10)
 
     part_cp = sems.copy(partial_s, partner_part, partner)
     wd_cp = sems.copy(dd_h.at[:, pl.ds(ohalf, 1024)], wd.at[pl.ds(ccol, 128)], partner)
-
-    def meta_copy(d):
-        return pltpu.make_async_remote_copy(
-            src_ref=meta_s,
-            dst_ref=meta_all.at[me],
-            send_sem=meta_sems.at[0],
-            recv_sem=meta_sems.at[1],
-            device_id=(d, core),
-            device_id_type=MESH,
-        )
 
     part_cp.wait_recv()
     attn = partial_s[...].astype(f32) + partner_part[...].astype(f32)
@@ -246,22 +235,28 @@
     pn_s[...] = post
     a1[:, 0] = pn_s[:, :, pl.ds(half, 1024)]
 
+    def meta_stage(dim, size):
+        return [
+            sems.copy(meta_all.at[pl.ds(0, size)], meta_all.at[pl.ds((4 - k) * size, size)], peer(dim, k))
+            for k in (1, 3, 2)
+        ]
+
+    meta_cp = meta_stage(0, 1)
     g1 = [
         [sems.copy(a1.at[p, 0], a1.at[p, 4 - k], peer(p, k)) for k in (1, 3, 2)]
         for p in range(3)
     ]
 
-    @pl.loop(1, 64)
-    def _(i):
-        meta_copy((me + i) % 64).start()
-
-    meta_all[me] = meta_s[...]
     branch = jax.nn.sigmoid(
         jnp.sum(post.astype(f32) * rows_s[pl.ds(2, 1), :][None], axis=-1, keepdims=True)
     )
 
     g2 = []
     for p in range(3):
+        if p == 0:
+            for cp in meta_cp:
+                cp.wait_recv()
+            meta_cp = meta_stage(1, 4)
         for cp in g1[p]:
             cp.wait_recv()
         for pair in range(2):
@@ -281,26 +276,30 @@
         view = xs.at[core, slot, pl.ds(p * 128 + start, size)]
         d2d[slot].append(sems.copy(view, view, partner))
 
-    for p in range(3):
+    lo, hi = (lambda p: pl.ds(p * 128, 64)), (lambda p: pl.ds(p * 128 + 64, 64))
+    for p in range(3):
+        if p == 0:
+            for cp in meta_cp:
+                cp.wait_recv()
+            meta_cp = meta_stage(2, 16)
         for cp in g2[p]:
             cp.wait_recv()
         cdim = (p + 2) % 3
-        rows = pl.ds(p * 128, 128)
-        g3.append((
-            sems.copy(xs.at[core, 0, rows], xs.at[core, 1, rows], peer(cdim, 1)),
-            sems.copy(xs.at[core, 0, rows], xs.at[core, 2, rows], peer(cdim, 3)),
-        ))
+        own = xs.at[core, 0]
+        g3.append([
+            sems.copy(own.at[rows], xs.at[core, slot, rows], peer(cdim, k))
+            for slot, k, rows in ((1, 1, lo(p)), (2, 3, hi(p)), (1, 1, hi(p)), (2, 3, lo(p)))
+        ])
         share(0, p, 0, 128)
 
-    pltpu.make_async_copy(
-        meta_all.at[pl.ds(0, 63)], meta_all.at[pl.ds(0, 63)], meta_sems.at[1]
-    ).wait()
+    for cp in meta_cp:
+        cp.wait_recv()
     for d in range(64):
         meta_tab[pl.ds(d, 1), :] = meta_all[d]
     table = meta_tab[...].astype(jnp.int32)
     lane = lax.broadcasted_iota(jnp.int32, (64, 128), 1)
     dev = lax.broadcasted_iota(jnp.int32, (64, 1), 0)
-    shift = [((dev >> s) - coords[i]) & 3 for i, s in enumerate((0, 2, 4))]
+    shift = [(dev >> s) & 3 for s in (0, 2, 4)]
     starts = []
     for p in range(3):
         ka, kb, kc = shift[p], shift[(p + 1) % 3], shift[(p + 2) % 3]
@@ -360,13 +359,16 @@
     for p in range(3):
         cdim = (p + 2) % 3
         g3[p][0].wait_recv()
-        rows = pl.ds(p * 128, 64)
-        relay.append(sems.copy(xs.at[core, 1, rows], xs.at[core, 3, rows], peer(cdim, 1)))
-        share(1, p, 0, 128)
+        relay.append(sems.copy(xs.at[core, 1, lo(p)], xs.at[core, 3, lo(p)], peer(cdim, 1)))
         g3[p][1].wait_recv()
-        rows = pl.ds(p * 128 + 64, 64)
-        relay.append(sems.copy(xs.at[core, 2, rows], xs.at[core, 3, rows], peer(cdim, 3)))
-        share(2, p, 0, 128)
+        relay.append(sems.copy(xs.at[core, 2, hi(p)], xs.at[core, 3, hi(p)], peer(cdim, 3)))
+        share(1, p, 0, 64)
+        share(2, p, 64, 64)
+    for p in range(3):
+        g3[p][2].wait_recv()
+        share(1, p, 64, 64)
+        g3[p][3].wait_recv()
+        share(2, p, 0, 64)
 
     arrive(1)
     up_proj(1)
@@ -383,8 +385,8 @@
     for p in range(3):
         cdim = (p + 2) % 3
         s1.append([
-            sems.copy(dens.at[2, pl.ds(p * 128 + 64, 64)], rl.at[p, 1], peer(cdim, 1)),
-            sems.copy(dens.at[1, pl.ds(p * 128, 64)], rr.at[p, 0], peer(cdim, 3)),
+            sems.copy(dens.at[2, hi(p)], rl.at[p, hi(0)], peer(cdim, 1)),
+            sems.copy(dens.at[1, lo(p)], rr.at[p, lo(0)], peer(cdim, 3)),
         ])
 
     for p in range(3):
@@ -399,10 +401,10 @@
     far = []
     for p in range(3):
         cdim = (p + 2) % 3
-        far.append((
-            sems.copy(dens.at[3, pl.ds(p * 128, 64)], ql.at[p], peer(cdim, 1)),
-            sems.copy(dens.at[3, pl.ds(p * 128 + 64, 64)], qr.at[p], peer(cdim, 3)),
-        ))
+        far.append([
+            sems.copy(dens.at[3, pl.ds(p * 128 + q * 32, 32)], buf.at[p, q % 2], peer(cdim, k))
+            for q, buf, k in ((1, ql, 1), (2, qr, 3), (0, ql, 1), (3, qr, 3))
+        ])
         s1[p] += [
             sems.copy(sq.at[2, p], sq1.at[p, 0], peer(cdim, 1)),
             sems.copy(sq.at[1, p], sq1.at[p, 1], peer(cdim, 3)),
@@ -421,14 +423,17 @@
     ep_cp = sems.copy(ep_send, ep_recv, partner)
     mine = jnp.dot(act, ed[:, pl.ds(half, 1024)], preferred_element_type=f32).astype(bf16)
 
-    for p in range(3):
-        cdim = (p + 2) % 3
-        far[p][0].wait_recv()
-        sl[p] = (dens[2, pl.ds(p * 128, 64)].astype(f32) + ql[p].astype(f32)).astype(bf16)
-        s1[p].append(sems.copy(sl.at[p], rl.at[p, 0], peer(cdim, 1)))
-        far[p][1].wait_recv()
-        sr[p] = (dens[1, pl.ds(p * 128 + 64, 64)].astype(f32) + qr[p].astype(f32)).astype(bf16)
-        s1[p].append(sems.copy(sr.at[p], rr.at[p, 1], peer(cdim, 3)))
+    sums = [[None] * 4 for _ in range(3)]
+    for i, (q, near, came, out, to, k) in enumerate((
+        (1, 2, ql, sl, rl, 1), (2, 1, qr, sr, rr, 3), (0, 2, ql, sl, rl, 1), (3, 1, qr, sr, rr, 3)
+    )):
+        for p in range(3):
+            far[p][i].wait_recv()
+            mix = dens[near, pl.ds(p * 128 + q * 32, 32)].astype(f32) + came[p, q % 2].astype(f32)
+            out[p, q % 2] = mix.astype(bf16)
+            sums[p][q] = sems.copy(
+                out.at[p, q % 2], to.at[p, pl.ds(q * 32, 32)], peer((p + 2) % 3, k)
+            )
 
     ep_cp.wait_recv()
     rows = (mine.astype(f32) + ep_recv[...].astype(f32)).astype(bf16).astype(f32)
@@ -437,41 +442,39 @@
             ret_f[pl.ds(s * 8 + t, 64, stride=16), :] = rows[s * 64:(s + 1) * 64, t * 128:(t + 1) * 128]
     ret_b[...] = ret_f[...].astype(bf16).reshape(64, 16, 128)
 
-    def back_copy(d):
-        return pltpu.make_async_remote_copy(
-            src_ref=ret_b.at[d],
+    @pl.loop(1, 64)
+    def _(i):
+        owner = (coords[0] + i % 4) % 4 + (coords[1] + (i // 4) % 4) % 4 * 4 + (coords[2] + i // 16) % 4 * 16
+        pltpu.make_async_remote_copy(
+            src_ref=ret_b.at[i],
             dst_ref=back.at[me],
             send_sem=back_sems.at[0],
             recv_sem=back_sems.at[1],
-            device_id=(d, core),
+            device_id=(owner, core),
             device_id_type=MESH,
-        )
-
-    @pl.loop(1, 64)
-    def _(i):
-        back_copy((me + i) % 64).start()
-
-    back[me] = ret_b[me]
+        ).start()
+
+    back[me] = ret_b[0]
     down_proj(0)
 
-    s2 = []
+    s2 = [[] for _ in range(3)]
     for p in range(3):
         for cp in s1[p]:
             cp.wait_recv()
-        total = dens[0, pl.ds(p * 128, 128)].astype(f32)
-        total = total + jnp.concatenate([rl[p, 0], rl[p, 1]], axis=0).astype(f32)
-        total = total + jnp.concatenate([rr[p, 0], rr[p, 1]], axis=0).astype(f32)
-        for k in range(4):
-            t2[p, k] = total[k * 32:(k + 1) * 32].astype(bf16)
         v = sq[0, p] + sq1[p, 0] + sq1[p, 1] + sq1[p, 2]
         sq2[p, 0] = v
         for k in range(1, 4):
             sq2[p, k] = pltpu.roll(v, 128 - 32 * k, 1)
-        s2.append([
-            sems.copy(t2.at[p, k], r2.at[p, k - 1], peer((p + 1) % 3, k)) for k in (1, 3, 2)
-        ] + [
-            sems.copy(sq2.at[p, k], sq2r.at[p, k - 1], peer((p + 1) % 3, k)) for k in (1, 3, 2)
-        ])
+            s2[p].append(sems.copy(sq2.at[p, k], sq2r.at[p, k - 1], peer((p + 1) % 3, k)))
+    for q in (2, 1, 3, 0):
+        for p in range(3):
+            sums[p][q].wait_recv()
+            rows = pl.ds(q * 32, 32)
+            total = dens[0, pl.ds(p * 128 + q * 32, 32)].astype(f32)
+            total = total + rl[p, rows].astype(f32) + rr[p, rows].astype(f32)
+            t2[p, q] = total.astype(bf16)
+            if q:
+                s2[p].append(sems.copy(t2.at[p, q], r2.at[p, q - 1], peer((p + 1) % 3, q)))
 
     pltpu.make_async_copy(back.at[pl.ds(0, 63)], back.at[pl.ds(0, 63)], back_sems.at[1]).wait()
     ret_f[...] = back[...].reshape(1024, 128).astype(f32)
@@ -521,9 +524,6 @@
 
     for cp in sems.sent:
         cp.wait_send()
-    pltpu.make_async_copy(
-        meta_all.at[pl.ds(0, 63)], meta_all.at[pl.ds(0, 63)], meta_sems.at[0]
-    ).wait()
     pltpu.make_async_copy(back.at[pl.ds(0, 63)], back.at[pl.ds(0, 63)], back_sems.at[0]).wait()
 
 
@@ -555,7 +555,6 @@
         V((24, 64), f32),
         V((192, 128), f32),
         V((24, 512), f32),
-        V((1, 128), f32),
         V((2, 24, 64), f32),
         V((3, 8, 2048), bf16),
         V((3, 8, 2048), bf16),
@@ -573,12 +572,12 @@
         V((64, 128), f32),
         V((2, 128, 1024), f32),
         V((4, 384, 1024), bf16),
-        V((3, 2, 64, 1024), bf16),
-        V((3, 2, 64, 1024), bf16),
-        V((3, 64, 1024), bf16),
-        V((3, 64, 1024), bf16),
-        V((3, 64, 1024), bf16),
-        V((3, 64, 1024), bf16),
+        V((3, 128, 1024), bf16),
+        V((3, 128, 1024), bf16),
+        V((3, 2, 32, 1024), bf16),
+        V((3, 2, 32, 1024), bf16),
+        V((3, 2, 32, 1024), bf16),
+        V((3, 2, 32, 1024), bf16),
         V((3, 4, 32, 1024), bf16),
         V((3, 3, 32, 1024), bf16),
         V((3, 4, 8, 1024), bf16),
@@ -594,12 +593,11 @@
         V((1024, 128), f32),
         V((64, 16, 128), bf16),
         V((64, 16, 128), bf16),
-        pltpu.SemaphoreType.DMA((128,)),
-        pltpu.SemaphoreType.DMA((128,)),
+        pltpu.SemaphoreType.DMA((192,)),
+        pltpu.SemaphoreType.DMA((192,)),
         pltpu.SemaphoreType.DMA((7,)),
         pltpu.SemaphoreType.DMA((13,)),
         pltpu.SemaphoreType.DMA((3, 6)),
-        pltpu.SemaphoreType.DMA((2,)),
         pltpu.SemaphoreType.DMA((2,)),
     ]
     return pl.pallas_call(
@@ -617,6 +615,19 @@
             collective_id=0, has_side_effects=True, vmem_limit_bytes=56 * 1024 * 1024
         ),
     )(lens, *args)
+
+
+def finish(*arrays):
+    def kernel(*refs):
+        for src, dst in zip(refs[:4], refs[4:]):
+            dst[...] = src[...]
+
+    return pl.pallas_call(
+        kernel,
+        out_shape=tuple(jax.ShapeDtypeStruct(a.shape, a.dtype) for a in arrays),
+        in_specs=[pl.BlockSpec(memory_space=pltpu.VMEM)] * 4,
+        out_specs=(pl.BlockSpec(memory_space=pltpu.VMEM),) * 4,
+    )(*arrays)
 
 
 def body(
@@ -671,8 +682,11 @@
         expert_up_w.reshape(2048, 512),
         expert_down_w.reshape(512, 2048),
     )
+    mixed, fresh_key, fresh_value, fresh_gate = finish(
+        mixed.reshape(24, 1024), fresh_key, fresh_value, fresh_gate
+    )
     return (
-        mixed.reshape(24, 1024),
+        mixed,
         fresh_key.reshape(24, 1, 64),
         fresh_value.reshape(24, 1, 64),
         fresh_gate.T,

time: 77.9 us -> 71.4 us (0.917)
  local copies, waits for them, and re-layouts: 5.27 us -> 0 us
  Pallas kernels: 71.7 us -> 70.5 us
    unnamed x4 -> x0, local copies, waits for them, and re-layouts: 5.27 us -> none
    pallas_call x1, Pallas kernels: 71.7 us -> 69.1 us  [fused_layer(): pl.pallas_call(layer_kernel, out_shape=(jax.ShapeDtypeStruct((3, 8, 1024)...]
    pallas_call x0 -> x1, Pallas kernels: none -> 1.45 us  [finish(): pl.pallas_call(kernel, out_shape=tuple((jax.ShapeDtypeStruct(a.shape, a.d...]
where the time goes in v3:
time: 71.4 us; the launch traced here: 71.2 us
  Pallas kernels  70.5 us (99%)
    pallas_call x1, Pallas kernels, fused_layer(): pl.pallas_call(layer_kernel, out_shape=(jax.ShapeDtypeStruct((3, 8, 1024)...  69.1 us
    pallas_call x1, Pallas kernels, finish(): pl.pallas_call(kernel, out_shape=tuple((jax.ShapeDtypeStruct(a.shape, a.d...  1.45 us

profile of v3, /device:TPU:0, one launch (start us, length us, event | category | flops | bytes accessed | tf_op | source)
XLA Modules:
  0.0 71.2 jit_solution(9694500467000103505)
XLA Ops:
  0.6 69.1 %shard_map.255 = (bf16[3,8,1024]{2,1,0:T(8,128)(2,1)}, bf16[24,64]{1,0:T(8,128)(2,1)}, bf16[24,64]{1,0:T(8,128)(2,1)}, f32[8,24]{1,0:T(8,128)}) custom-call(s32[24]{0:T(128)} %len_ref.1, bf16[24,2048]{1,0:T(8,128)(2,1)} %tokens_h.1, bf16[16,128]{1,0:T(8,128)(2,1)} %bitcast.25, bf16[16,128]{1,0:T(8,128)(2,1)} %bitcast.26, bf16[16,128]{1,0:T(8,128)(2,1)} %bitcast.27, ...), custom_call_target="tpu_custom_call" | custom-call | tf_op jit(solution)/shard_map/pallas_call | solution.py:603
  69.7 1.5 %shard_map.256 = (bf16[24,1024]{1,0:T(8,128)(2,1)}, bf16[24,64]{1,0:T(8,128)(2,1)}, bf16[24,64]{1,0:T(8,128)(2,1)}, f32[8,24]{1,0:T(8,128)}) custom-call(bf16[24,1024]{1,0:T(8,128)(2,1)} %bitcast.24, bf16[24,64]{1,0:T(8,128)(2,1)} %get-tuple-element.13.refs_1_, bf16[24,64]{1,0:T(8,128)(2,1)} %get-tuple-element.14.refs_2_, f32[8,24]{1,0:T(8,128)} %get-tuple-element.15.refs_3_), custom_call_target="tpu_custom_call" | custom-call | tf_op jit(solution)/shard_map/pallas_call | solution.py:625

commit v4 on v3

--- a/solution.py
+++ b/solution.py
@@ -10,6 +10,7 @@
 
 FF2 = 16384
 norm_eps = 1e-06
+GROUP = 8
 MESH = pl.DeviceIdType.MESH
 f32, bf16 = jnp.float32, jnp.bfloat16
 
@@ -85,7 +86,7 @@
         smalls.append(cp)
 
     def cache_copies(g):
-        rows = pl.ds(g * 4, 4)
+        rows = pl.ds(g * GROUP, GROUP)
         return [
             pltpu.make_async_copy(src.at[rows], dst.at[rows], cache_sem.at[i, g])
             for i, (src, dst) in enumerate(((kc_h, kc), (cg_h, cg), (vc_h, vc)))
@@ -130,7 +131,7 @@
         comb_s[t] = m + jnp.where(target_col[1] == place + t, weight_col[1], 0.0)
 
     smalls[4].wait()
-    for g in range(6):
+    for g in range(24 // GROUP):
         for cp in cache_copies(g):
             cp.start()
     loads[6].start()
@@ -180,11 +181,11 @@
     seq_lane = lax.broadcasted_iota(jnp.int32, (8, 24), 1)
     scale = 64 ** (-0.5)
 
-    def attend(g, gates):
+    def score_group(g, gates):
         for cp in cache_copies(g):
             cp.wait()
-        for i in range(4):
-            s = g * 4 + i
+        for i in range(GROUP):
+            s = g * GROUP + i
             rows = pl.ds(pl.multiple_of(s * 8, 8), 8)
             length = len_ref[s]
             q = q_s[rows, :][:, :64]
@@ -198,19 +199,26 @@
             own = jnp.sum(q * kf_s[pl.ds(s, 1), :], axis=1, keepdims=True) * scale
             logit = jnp.where(slot_at < length, score + (current - gate), -jnp.inf)
             top = jnp.maximum(jnp.max(logit, axis=1, keepdims=True), own)
-            w = jnp.exp(logit - top)
-            own_w = jnp.exp(own - top)
+            cg[s] = logit - top
+            o_s[rows, :] = jnp.broadcast_to(own - top, (8, 128))
+        return gates
+
+    def mix_group(g, carry):
+        for i in range(GROUP):
+            s = g * GROUP + i
+            rows = pl.ds(pl.multiple_of(s * 8, 8), 8)
+            w = jnp.exp(cg[s])
+            own_w = jnp.exp(o_s[rows, :][:, :64])
             inv = 1.0 / (jnp.sum(w, axis=1, keepdims=True) + own_w)
-            probs = (w * inv).astype(bf16)
-            own_p = (own_w * inv).astype(bf16).astype(f32)
             o = lax.dot_general(
-                probs, vc[s], (((1,), (1,)), ((), ())), preferred_element_type=f32
+                w.astype(bf16), vc[s], (((1,), (1,)), ((), ())), preferred_element_type=f32
             )
-            o = o + own_p * vf_s[pl.ds(s, 1), :]
+            o = (o + own_w.astype(bf16).astype(f32) * vf_s[pl.ds(s, 1), :]) * inv
             o_s[rows, :] = jnp.concatenate([o, jnp.zeros_like(o)], axis=1)
-        return gates
-
-    gates = lax.fori_loop(0, 6, attend, jnp.zeros((8, 24), f32))
+        return carry
+
+    gates = lax.fori_loop(0, 24 // GROUP, score_group, jnp.zeros((8, 24), f32))
+    lax.fori_loop(0, 24 // GROUP, mix_group, 0)
     fg_ref[...] = gates
     for cp in loads[:6]:
         cp.start()
@@ -336,9 +344,10 @@
 
     def down_proj(slot):
         h_cp[slot].wait_recv()
-        h = hid[slot]
-        hf = h.astype(f32)
-        dens[slot] = jnp.dot(h, wd[...], preferred_element_type=f32).astype(bf16)
+        dens[slot] = jnp.dot(hid[slot], wd[...], preferred_element_type=f32).astype(bf16)
+
+    def squares(slot):
+        hf = hid[slot].astype(f32)
         s = lax.dot_general(
             ones, (hf * hf).astype(bf16), (((1,), (1,)), ((), ())), preferred_element_type=f32
         )
@@ -376,9 +385,12 @@
     up_proj(2)
     loads[2].wait()
     wd_cp.wait_recv()
-    select(1)
     down_proj(1)
-    select(2)
+    for p in range(3):
+        relay[2 * p].wait_recv()
+        share(3, p, 0, 64)
+        relay[2 * p + 1].wait_recv()
+        share(3, p, 64, 64)
     down_proj(2)
 
     s1 = []
@@ -389,14 +401,10 @@
             sems.copy(dens.at[1, lo(p)], rr.at[p, lo(0)], peer(cdim, 3)),
         ])
 
-    for p in range(3):
-        relay[2 * p].wait_recv()
-        share(3, p, 0, 64)
-        relay[2 * p + 1].wait_recv()
-        share(3, p, 64, 64)
     arrive(3)
     up_proj(3)
-    select(3)
+    select(1)
+    select(2)
     down_proj(3)
     far = []
     for p in range(3):
@@ -405,6 +413,11 @@
             sems.copy(dens.at[3, pl.ds(p * 128 + q * 32, 32)], buf.at[p, q % 2], peer(cdim, k))
             for q, buf, k in ((1, ql, 1), (2, qr, 3), (0, ql, 1), (3, qr, 3))
         ])
+    select(3)
+    for slot in (1, 2, 3):
+        squares(slot)
+    for p in range(3):
+        cdim = (p + 2) % 3
         s1[p] += [
             sems.copy(sq.at[2, p], sq1.at[p, 0], peer(cdim, 1)),
             sems.copy(sq.at[1, p], sq1.at[p, 1], peer(cdim, 3)),
@@ -423,6 +436,9 @@
     ep_cp = sems.copy(ep_send, ep_recv, partner)
     mine = jnp.dot(act, ed[:, pl.ds(half, 1024)], preferred_element_type=f32).astype(bf16)
 
+    down_proj(0)
+    squares(0)
+
     sums = [[None] * 4 for _ in range(3)]
     for i, (q, near, came, out, to, k) in enumerate((
         (1, 2, ql, sl, rl, 1), (2, 1, qr, sr, rr, 3), (0, 2, ql, sl, rl, 1), (3, 1, qr, sr, rr, 3)
@@ -441,21 +457,6 @@
         for t in range(8):
             ret_f[pl.ds(s * 8 + t, 64, stride=16), :] = rows[s * 64:(s + 1) * 64, t * 128:(t + 1) * 128]
     ret_b[...] = ret_f[...].astype(bf16).reshape(64, 16, 128)
-
-    @pl.loop(1, 64)
-    def _(i):
-        owner = (coords[0] + i % 4) % 4 + (coords[1] + (i // 4) % 4) % 4 * 4 + (coords[2] + i // 16) % 4 * 16
-        pltpu.make_async_remote_copy(
-            src_ref=ret_b.at[i],
-            dst_ref=back.at[me],
-            send_sem=back_sems.at[0],
-            recv_sem=back_sems.at[1],
-            device_id=(owner, core),
-            device_id_type=MESH,
-        ).start()
-
-    back[me] = ret_b[0]
-    down_proj(0)
 
     s2 = [[] for _ in range(3)]
     for p in range(3):
@@ -476,19 +477,19 @@
             if q:
                 s2[p].append(sems.copy(t2.at[p, q], r2.at[p, q - 1], peer((p + 1) % 3, q)))
 
-    pltpu.make_async_copy(back.at[pl.ds(0, 63)], back.at[pl.ds(0, 63)], back_sems.at[1]).wait()
-    ret_f[...] = back[...].reshape(1024, 128).astype(f32)
-    mixes = []
-    for t in range(8):
-        m = 0.0
-        for s in range(2):
-            m = m + jnp.dot(
-                comb_s[s], ret_f[pl.ds(s * 8 + t, 64, stride=16), :],
-                preferred_element_type=f32, precision=lax.Precision.HIGHEST,
-            )
-        mixes.append(m)
-    expert_sum = jnp.concatenate(mixes, axis=1)
-
+    @pl.loop(1, 64)
+    def _(i):
+        owner = (coords[0] + i % 4) % 4 + (coords[1] + (i // 4) % 4) % 4 * 4 + (coords[2] + i // 16) % 4 * 16
+        pltpu.make_async_remote_copy(
+            src_ref=ret_b.at[i],
+            dst_ref=back.at[me],
+            send_sem=back_sems.at[0],
+            recv_sem=back_sems.at[1],
+            device_id=(owner, core),
+            device_id_type=MESH,
+        ).start()
+
+    back[me] = ret_b[0]
     s3 = []
     for p in range(3):
         for cp in s2[p]:
@@ -507,6 +508,19 @@
         ] + [
             sems.copy(sq3.at[p, k], sq3r.at[p, k - 1], peer(p, k)) for k in (1, 3, 2)
         ])
+
+    pltpu.make_async_copy(back.at[pl.ds(0, 63)], back.at[pl.ds(0, 63)], back_sems.at[1]).wait()
+    ret_f[...] = back[...].reshape(1024, 128).astype(f32)
+    mixes = []
+    for t in range(8):
+        m = 0.0
+        for s in range(2):
+            m = m + jnp.dot(
+                comb_s[s], ret_f[pl.ds(s * 8 + t, 64, stride=16), :],
+                preferred_element_type=f32, precision=lax.Precision.HIGHEST,
+            )
+        mixes.append(m)
+    expert_sum = jnp.concatenate(mixes, axis=1)
 
     eye = lax.broadcasted_iota(jnp.int32, (8, 128), 0) == lax.broadcasted_iota(jnp.int32, (8, 128), 1)
     for p in range(3):
@@ -597,16 +611,16 @@
         pltpu.SemaphoreType.DMA((192,)),
         pltpu.SemaphoreType.DMA((7,)),
         pltpu.SemaphoreType.DMA((13,)),
-        pltpu.SemaphoreType.DMA((3, 6)),
+        pltpu.SemaphoreType.DMA((3, 24 // GROUP)),
         pltpu.SemaphoreType.DMA((2,)),
     ]
     return pl.pallas_call(
         layer_kernel,
         out_shape=(
-            jax.ShapeDtypeStruct((3, 8, 1024), bf16),
-            jax.ShapeDtypeStruct((24, 64), bf16),
-            jax.ShapeDtypeStruct((24, 64), bf16),
-            jax.ShapeDtypeStruct((8, 24), f32),
+            pltpu.VMEM((3, 8, 1024), bf16),
+            pltpu.VMEM((24, 64), bf16),
+            pltpu.VMEM((24, 64), bf16),
+            pltpu.VMEM((8, 24), f32),
         ),
         in_specs=[pl.BlockSpec(memory_space=pltpu.SMEM)] + [hbm] * len(args),
         out_specs=(vm,) * 4,

time: 71.4 us -> 68 us (0.952)
  Pallas kernels: 70.5 us -> 64.8 us
  local copies, waits for them, and re-layouts: 0 us -> 2.38 us
    pallas_call x1, Pallas kernels: 69.1 us -> 63.4 us  [fused_layer(): pl.pallas_call(layer_kernel, out_shape=(pltpu.VMEM((3, 8, 1024), bf16), p...]
    unnamed x0 -> x8, local copies, waits for them, and re-layouts: none -> 2.38 us
where the time goes in v4:
time: 68 us; the launch traced here: 67.9 us
  Pallas kernels  64.8 us (95%)
  local copies, waits for them, and re-layouts  2.38 us (4%)
    pallas_call x1, Pallas kernels, fused_layer(): pl.pallas_call(layer_kernel, out_shape=(pltpu.VMEM((3, 8, 1024), bf16), p...  63.4 us
    unnamed x8, local copies, waits for them, and re-layouts  2.38 us
    pallas_call x1, Pallas kernels, finish(): pl.pallas_call(kernel, out_shape=tuple((jax.ShapeDtypeStruct(a.shape, a.d...  1.45 us

profile of v4, /device:TPU:0, one launch (start us, length us, event | category | flops | bytes accessed | tf_op | source)
XLA Modules:
  0.0 67.9 jit_solution(17679206907197311854)
XLA Ops:
  0.6 63.4 %shard_map.255 = (bf16[3,8,1024]{2,1,0:T(8,128)(2,1)S(1)}, bf16[24,64]{1,0:T(8,128)(2,1)S(1)}, bf16[24,64]{1,0:T(8,128)(2,1)S(1)}, f32[8,24]{1,0:T(8,128)S(1)}) custom-call(s32[24]{0:T(128)} %len_ref.1, bf16[24,2048]{1,0:T(8,128)(2,1)} %tokens_h.1, bf16[16,128]{1,0:T(8,128)(2,1)} %bitcast.25, bf16[16,128]{1,0:T(8,128)(2,1)} %bitcast.26, ...), custom_call_target="tpu_custom_call" | custom-call | tf_op jit(solution)/shard_map/pallas_call | solution.py:617
  64.0 0.0 copy-start
  64.0 0.6 copy-done
  64.6 0.0 copy-start.1
  64.6 0.6 copy-done.1
  65.2 0.0 copy-start.2
  65.2 0.6 copy-done.2
  65.8 0.0 copy-start.3
  65.8 0.6 copy-done.3
  66.4 1.4 %shard_map.256 = (bf16[24,1024]{1,0:T(8,128)(2,1)}, bf16[24,64]{1,0:T(8,128)(2,1)}, bf16[24,64]{1,0:T(8,128)(2,1)}, f32[8,24]{1,0:T(8,128)}) custom-call(bf16[24,1024]{1,0:T(8,128)(2,1)} %bitcast.18, bf16[24,64]{1,0:T(8,128)(2,1)} %copy-done.1, bf16[24,64]{1,0:T(8,128)(2,1)} %copy-done.2, f32[8,24]{1,0:T(8,128)} %copy-done.3), custom_call_target="tpu_custom_call" | custom-call | tf_op jit(solution)/shard_map/pallas_call | solution.py:639
Async XLA Ops:
  64.0 0.6 copy-start
  64.6 0.6 copy-start.1
  65.2 0.6 copy-start.2
  65.8 0.6 copy-start.3

commit v5 on v4

--- a/solution.py
+++ b/solution.py
@@ -103,33 +103,6 @@
         (ow_h, ow),
     )):
         loads.append(pltpu.make_async_copy(src, dst, load_sem.at[i]))
-    meta_all[0] = jnp.full((1, 128), -1.0, f32)
-
-    def column(row):
-        pick = lax.broadcasted_iota(jnp.int32, (24, 24), 0) == lax.broadcasted_iota(jnp.int32, (24, 24), 1)
-        return jnp.sum(jnp.where(pick, row, jnp.zeros_like(row)), axis=1, keepdims=True)
-
-    smalls[2].wait()
-    smalls[3].wait()
-    choice = choice_s[...].astype(f32)
-    named = [choice[k:k + 1, :] for k in range(2)]
-    named_col = [column(v) for v in named]
-    earlier = lax.broadcasted_iota(jnp.int32, (24, 24), 0) < lax.broadcasted_iota(jnp.int32, (24, 24), 1)
-    targets = []
-    for k in range(2):
-        again = jnp.zeros((1, 24), f32)
-        for i in range(2):
-            same = jnp.where(earlier & (named_col[i] == named[k]), 1.0, 0.0)
-            again = again + jnp.sum(same, axis=0, keepdims=True)
-        targets.append(named[k] * 2.0 + jnp.minimum(again, 1.0))
-    meta_all[0, :, pl.ds(0, 24)] = targets[0] + 128.0 * targets[1]
-    target_col = [column(v) for v in targets]
-    weight_col = [column(rweight_s[k:k + 1, :]) for k in range(2)]
-    place = lax.broadcasted_iota(jnp.int32, (24, 64), 1).astype(f32) * 2.0
-    for t in range(2):
-        m = jnp.where(target_col[0] == place + t, weight_col[0], 0.0)
-        comb_s[t] = m + jnp.where(target_col[1] == place + t, weight_col[1], 0.0)
-
     smalls[4].wait()
     for g in range(24 // GROUP):
         for cp in cache_copies(g):
@@ -233,6 +206,33 @@
     part_cp = sems.copy(partial_s, partner_part, partner)
     wd_cp = sems.copy(dd_h.at[:, pl.ds(ohalf, 1024)], wd.at[pl.ds(ccol, 128)], partner)
 
+    meta_all[0] = jnp.full((1, 128), -1.0, f32)
+
+    def column(row):
+        pick = lax.broadcasted_iota(jnp.int32, (24, 24), 0) == lax.broadcasted_iota(jnp.int32, (24, 24), 1)
+        return jnp.sum(jnp.where(pick, row, jnp.zeros_like(row)), axis=1, keepdims=True)
+
+    smalls[2].wait()
+    smalls[3].wait()
+    choice = choice_s[...].astype(f32)
+    named = [choice[k:k + 1, :] for k in range(2)]
+    named_col = [column(v) for v in named]
+    earlier = lax.broadcasted_iota(jnp.int32, (24, 24), 0) < lax.broadcasted_iota(jnp.int32, (24, 24), 1)
+    targets = []
+    for k in range(2):
+        again = jnp.zeros((1, 24), f32)
+        for i in range(2):
+            same = jnp.where(earlier & (named_col[i] == named[k]), 1.0, 0.0)
+            again = again + jnp.sum(same, axis=0, keepdims=True)
+        targets.append(named[k] * 2.0 + jnp.minimum(again, 1.0))
+    meta_all[0, :, pl.ds(0, 24)] = targets[0] + 128.0 * targets[1]
+    target_col = [column(v) for v in targets]
+    weight_col = [column(rweight_s[k:k + 1, :]) for k in range(2)]
+    place = lax.broadcasted_iota(jnp.int32, (24, 64), 1).astype(f32) * 2.0
+    for t in range(2):
+        m = jnp.where(target_col[0] == place + t, weight_col[0], 0.0)
+        comb_s[t] = m + jnp.where(target_col[1] == place + t, weight_col[1], 0.0)
+
     part_cp.wait_recv()
     attn = partial_s[...].astype(f32) + partner_part[...].astype(f32)
     resid = (tok_s[...].astype(f32).reshape(3, 8, 2048) + attn).astype(bf16).astype(f32)
@@ -285,6 +285,15 @@
         d2d[slot].append(sems.copy(view, view, partner))
 
     lo, hi = (lambda p: pl.ds(p * 128, 64)), (lambda p: pl.ds(p * 128 + 64, 64))
+    first, second = (lambda p: pl.ds(p * 128, 32)), (lambda p: pl.ds(p * 128 + 32, 32))
+    own = xs.at[core, 0]
+    early = [
+        [
+            sems.copy(own.at[first(p)], xs.at[core, slot, first(p)], peer((p + 2) % 3, k))
+            for slot, k in ((1, 1), (2, 3))
+        ]
+        for p in range(3)
+    ]
     for p in range(3):
         if p == 0:
             for cp in meta_cp:
@@ -293,10 +302,9 @@
         for cp in g2[p]:
             cp.wait_recv()
         cdim = (p + 2) % 3
-        own = xs.at[core, 0]
         g3.append([
             sems.copy(own.at[rows], xs.at[core, slot, rows], peer(cdim, k))
-            for slot, k, rows in ((1, 1, lo(p)), (2, 3, hi(p)), (1, 1, hi(p)), (2, 3, lo(p)))
+            for slot, k, rows in ((1, 1, second(p)), (2, 3, hi(p)), (1, 1, hi(p)), (2, 3, second(p)))
         ])
         share(0, p, 0, 128)
 
@@ -342,6 +350,14 @@
 
     ones = jnp.ones((8, 256), bf16)
 
+    def far_up(p):
+        rows = pl.ds(p * 128, 128)
+        v = jnp.dot(xs[0, 3, rows], wgu[pl.ds(0, 1024)], preferred_element_type=f32)
+        v = v + jnp.dot(xs[1, 3, rows], wgu[pl.ds(1024, 1024)], preferred_element_type=f32)
+        hid[3, rows, pl.ds(ccol, 128)] = (silu(v[:, :128]) * v[:, 128:]).astype(bf16)
+        view = hid.at[3, rows, pl.ds(ccol, 128)]
+        return sems.copy(view, view, partner)
+
     def down_proj(slot):
         h_cp[slot].wait_recv()
         dens[slot] = jnp.dot(hid[slot], wd[...], preferred_element_type=f32).astype(bf16)
@@ -367,6 +383,7 @@
     relay = []
     for p in range(3):
         cdim = (p + 2) % 3
+        early[p][0].wait_recv()
         g3[p][0].wait_recv()
         relay.append(sems.copy(xs.at[core, 1, lo(p)], xs.at[core, 3, lo(p)], peer(cdim, 1)))
         g3[p][1].wait_recv()
@@ -376,6 +393,7 @@
     for p in range(3):
         g3[p][2].wait_recv()
         share(1, p, 64, 64)
+        early[p][1].wait_recv()
         g3[p][3].wait_recv()
         share(2, p, 0, 64)
 
@@ -401,14 +419,19 @@
             sems.copy(dens.at[1, lo(p)], rr.at[p, lo(0)], peer(cdim, 3)),
         ])
 
-    arrive(3)
-    up_proj(3)
+    far_cp = []
+    for p in range(3):
+        for cp in d2d[3][2 * p:2 * p + 2]:
+            cp.wait_recv()
+        far_cp.append(far_up(p))
     select(1)
     select(2)
-    down_proj(3)
     far = []
     for p in range(3):
         cdim = (p + 2) % 3
+        far_cp[p].wait_recv()
+        rows = pl.ds(p * 128, 128)
+        dens[3, rows] = jnp.dot(hid[3, rows], wd[...], preferred_element_type=f32).astype(bf16)
         far.append([
             sems.copy(dens.at[3, pl.ds(p * 128 + q * 32, 32)], buf.at[p, q % 2], peer(cdim, k))
             for q, buf, k in ((1, ql, 1), (2, qr, 3), (0, ql, 1), (3, qr, 3))
@@ -617,10 +640,10 @@
     return pl.pallas_call(
         layer_kernel,
         out_shape=(
-            pltpu.VMEM((3, 8, 1024), bf16),
-            pltpu.VMEM((24, 64), bf16),
-            pltpu.VMEM((24, 64), bf16),
-            pltpu.VMEM((8, 24), f32),
+            jax.ShapeDtypeStruct((3, 8, 1024), bf16),
+            jax.ShapeDtypeStruct((24, 64), bf16),
+            jax.ShapeDtypeStruct((24, 64), bf16),
+            jax.ShapeDtypeStruct((8, 24), f32),
         ),
         in_specs=[pl.BlockSpec(memory_space=pltpu.SMEM)] + [hbm] * len(args),
         out_specs=(vm,) * 4,

time: 68 us -> 64.1 us (0.943)
  local copies, waits for them, and re-layouts: 2.38 us -> 0 us
  Pallas kernels: 64.8 us -> 63.3 us
    unnamed x8 -> x0, local copies, waits for them, and re-layouts: 2.38 us -> none
    pallas_call x1, Pallas kernels: 63.4 us -> 61.8 us  [fused_layer(): pl.pallas_call(layer_kernel, out_shape=(jax.ShapeDtypeStruct((3, 8, 1024)...]
where the time goes in v5:
time: 64.1 us; the launch traced here: 63.9 us
  Pallas kernels  63.3 us (99%)
  between operations  0.65 us (1%)
    pallas_call x1, Pallas kernels, fused_layer(): pl.pallas_call(layer_kernel, out_shape=(jax.ShapeDtypeStruct((3, 8, 1024)...  61.8 us
    pallas_call x1, Pallas kernels, finish(): pl.pallas_call(kernel, out_shape=tuple((jax.ShapeDtypeStruct(a.shape, a.d...  1.45 us

profile of v5, /device:TPU:0, one launch (start us, length us, event | category | flops | bytes accessed | tf_op | source)
XLA Modules:
  0.0 63.9 jit_solution(7645334834898951321)
XLA Ops:
  0.6 61.8 %shard_map.255 = (bf16[3,8,1024]{2,1,0:T(8,128)(2,1)}, bf16[24,64]{1,0:T(8,128)(2,1)}, bf16[24,64]{1,0:T(8,128)(2,1)}, f32[8,24]{1,0:T(8,128)}) custom-call(s32[24]{0:T(128)} %len_ref.1, bf16[24,2048]{1,0:T(8,128)(2,1)} %tokens_h.1, bf16[16,128]{1,0:T(8,128)(2,1)} %bitcast.25, bf16[16,128]{1,0:T(8,128)(2,1)} %bitcast.26, bf16[16,128]{1,0:T(8,128)(2,1)} %bitcast.27, ...), custom_call_target="tpu_custom_call" | custom-call | tf_op jit(solution)/shard_map/pallas_call | solution.py:640
  62.5 1.5 %shard_map.256 = (bf16[24,1024]{1,0:T(8,128)(2,1)}, bf16[24,64]{1,0:T(8,128)(2,1)}, bf16[24,64]{1,0:T(8,128)(2,1)}, f32[8,24]{1,0:T(8,128)}) custom-call(bf16[24,1024]{1,0:T(8,128)(2,1)} %bitcast.24, bf16[24,64]{1,0:T(8,128)(2,1)} %get-tuple-element.13.refs_1_, bf16[24,64]{1,0:T(8,128)(2,1)} %get-tuple-element.14.refs_2_, f32[8,24]{1,0:T(8,128)} %get-tuple-element.15.refs_3_), custom_call_target="tpu_custom_call" | custom-call | tf_op jit(solution)/shard_map/pallas_call | solution.py:662

commit v6 on v5

--- a/solution.py
+++ b/solution.py
@@ -341,19 +341,24 @@
 
     h_cp = [None] * 4
 
-    def up_proj(slot):
-        v = jnp.dot(xs[0, slot], wgu[pl.ds(0, 1024)], preferred_element_type=f32)
-        v = v + jnp.dot(xs[1, slot], wgu[pl.ds(1024, 1024)], preferred_element_type=f32)
+    def half_up(h, slot, rows):
+        w = wgu[pl.ds(pl.multiple_of(h * 1024, 1024), 1024)]
+        return jnp.dot(xs[h, slot, rows], w, preferred_element_type=f32)
+
+    def own_up(slot):
+        return half_up(core, slot, pl.ds(0, 384))
+
+    def up_proj(slot, v):
+        v = v + half_up(other, slot, pl.ds(0, 384))
         hid[slot, :, pl.ds(ccol, 128)] = (silu(v[:, :128]) * v[:, 128:]).astype(bf16)
         view = hid.at[slot, :, pl.ds(ccol, 128)]
         h_cp[slot] = sems.copy(view, view, partner)
 
     ones = jnp.ones((8, 256), bf16)
 
-    def far_up(p):
+    def far_up(p, v):
         rows = pl.ds(p * 128, 128)
-        v = jnp.dot(xs[0, 3, rows], wgu[pl.ds(0, 1024)], preferred_element_type=f32)
-        v = v + jnp.dot(xs[1, 3, rows], wgu[pl.ds(1024, 1024)], preferred_element_type=f32)
+        v = v + half_up(other, 3, rows)
         hid[3, rows, pl.ds(ccol, 128)] = (silu(v[:, :128]) * v[:, 128:]).astype(bf16)
         view = hid.at[3, rows, pl.ds(ccol, 128)]
         return sems.copy(view, view, partner)
@@ -376,8 +381,9 @@
 
     loads[0].wait()
     loads[1].wait()
+    v0 = own_up(0)
     arrive(0)
-    up_proj(0)
+    up_proj(0, v0)
     select(0)
 
     relay = []
@@ -397,10 +403,11 @@
         g3[p][3].wait_recv()
         share(2, p, 0, 64)
 
+    v1, v2 = own_up(1), own_up(2)
     arrive(1)
-    up_proj(1)
+    up_proj(1, v1)
     arrive(2)
-    up_proj(2)
+    up_proj(2, v2)
     loads[2].wait()
     wd_cp.wait_recv()
     down_proj(1)
@@ -420,10 +427,11 @@
         ])
 
     far_cp = []
+    far_own = [half_up(core, 3, pl.ds(p * 128, 128)) for p in range(3)]
     for p in range(3):
         for cp in d2d[3][2 * p:2 * p + 2]:
             cp.wait_recv()
-        far_cp.append(far_up(p))
+        far_cp.append(far_up(p, far_own[p]))
     select(1)
     select(2)
     far = []

time: 64.1 us -> 64.1 us (level)
  no operation moved by 1% of the time
where the time goes in v6:
time: 64.1 us; the launch traced here: 63.9 us
  Pallas kernels  63.3 us (99%)
  between operations  0.65 us (1%)
    pallas_call x1, Pallas kernels, fused_layer(): pl.pallas_call(layer_kernel, out_shape=(jax.ShapeDtypeStruct((3, 8, 1024)...  61.8 us
    pallas_call x1, Pallas kernels, finish(): pl.pallas_call(kernel, out_shape=tuple((jax.ShapeDtypeStruct(a.shape, a.d...  1.45 us

profile of v6, /device:TPU:0, one launch (start us, length us, event | category | flops | bytes accessed | tf_op | source)
XLA Modules:
  0.0 63.9 jit_solution(10563695391434799192)
XLA Ops:
  0.6 61.8 %shard_map.255 = (bf16[3,8,1024]{2,1,0:T(8,128)(2,1)}, bf16[24,64]{1,0:T(8,128)(2,1)}, bf16[24,64]{1,0:T(8,128)(2,1)}, f32[8,24]{1,0:T(8,128)}) custom-call(s32[24]{0:T(128)} %len_ref.1, bf16[24,2048]{1,0:T(8,128)(2,1)} %tokens_h.1, bf16[16,128]{1,0:T(8,128)(2,1)} %bitcast.25, bf16[16,128]{1,0:T(8,128)(2,1)} %bitcast.26, bf16[16,128]{1,0:T(8,128)(2,1)} %bitcast.27, ...), custom_call_target="tpu_custom_call" | custom-call | tf_op jit(solution)/shard_map/pallas_call | solution.py:648
  62.5 1.5 %shard_map.256 = (bf16[24,1024]{1,0:T(8,128)(2,1)}, bf16[24,64]{1,0:T(8,128)(2,1)}, bf16[24,64]{1,0:T(8,128)(2,1)}, f32[8,24]{1,0:T(8,128)}) custom-call(bf16[24,1024]{1,0:T(8,128)(2,1)} %bitcast.24, bf16[24,64]{1,0:T(8,128)(2,1)} %get-tuple-element.13.refs_1_, bf16[24,64]{1,0:T(8,128)(2,1)} %get-tuple-element.14.refs_2_, f32[8,24]{1,0:T(8,128)} %get-tuple-element.15.refs_3_), custom_call_target="tpu_custom_call" | custom-call | tf_op jit(solution)/shard_map/pallas_call | solution.py:670
